TPU v7x, 768 devices: a whole 4x8x12 slice. The times are simulated.
768 devices in a mesh: sp: 192 (over z, y, core), tp: 4 (over x).
Axes of the slice: x: 4, y: 8, z: 12, core: 2. Of those that a mesh axis runs over, the one named last changes fastest.
Arguments:
- query_rows: bfloat16 [196608, 1024], P(('sp', 'tp')), may hold values from -6 to 6
- key_rows: bfloat16 [196608, 1024], P(('sp', 'tp')), may hold values from -6 to 6
- value_rows: bfloat16 [196608, 1024], P(('sp', 'tp')), may hold values from -6 to 6
- out_grad: bfloat16 [196608, 1024], P(('sp', 'tp')), may hold values from -40 to 40
- log_totals: float32 [196608, 8], P(('sp', 'tp')), may hold values from 6 to 7.5
- out_dot: float32 [196608, 8], P(('sp', 'tp')), may hold values from -6 to 6
- bias_table: float32 [8, 320], replicated, may hold values from -4 to 4
Outputs:
- grad_query: bfloat16 [196608, 1024], P(('sp', 'tp'))
- grad_key: bfloat16 [196608, 1024], P(('sp', 'tp'))
- grad_value: bfloat16 [196608, 1024], P(('sp', 'tp'))
- grad_table: float32 [8, 320], replicated
All inputs are finite; a program needn't handle non-finite values.
Results may differ from a plain program's by a relative error of at most 0.005.
Values may be sent and summed in bfloat16 or wider, within the bound.
A program may use at most 128 MiB of HBM per device.

v0:
```python
import functools

import jax
import jax.numpy as jnp
from jax import lax
from jax.sharding import Mesh
from jax.sharding import PartitionSpec as P

SEG_LEN = 64
LEFT_SEGS = 8
REL_CLIP = 256
SP_TP = ("sp_0", "sp_1", "sp_2", "tp")


def passed_along(block, axis, distance):
    devices = range(lax.axis_size(axis))
    route = [(i - distance, i) for i in devices if i - distance in devices]
    return lax.ppermute(block, axis, route)


def over_axes(shard, axes):
    return functools.reduce(lax.psum, axes, shard)


def band_matrix(diagonal_vals, row_count, col_count):
    head_count = diagonal_vals.shape[0]
    span_width = row_count + col_count - 1
    repeated = jnp.broadcast_to(diagonal_vals[:, None, :], (head_count, row_count, span_width))
    flat_rows = jnp.pad(
        repeated.reshape(head_count, row_count * span_width), ((0, 0), (0, row_count))
    )
    shaped = flat_rows.reshape(head_count, row_count, span_width + 1)[:, :, :col_count]
    return shaped[:, :, ::-1]


def diagonal_sums(matrix_vals):
    head_count, row_count, col_count = matrix_vals.shape
    span_width = row_count + col_count - 1
    flipped = jnp.pad(matrix_vals[:, :, ::-1], ((0, 0), (0, 0), (0, row_count)))
    skewed = flipped.reshape(head_count, row_count * (col_count + row_count))[
        :, : row_count * span_width
    ]
    return jnp.sum(skewed.reshape(head_count, row_count, span_width), axis=1)


def table_onehot(offset, row_count, col_count, table_len):
    diagonals = jnp.arange(row_count + col_count - 1, dtype=jnp.int32)
    distance = jnp.clip(offset + diagonals - (col_count - 1), 1 - SEG_LEN, REL_CLIP) + SEG_LEN - 1
    return (distance[:, None] == jnp.arange(table_len, dtype=jnp.int32)[None, :]).astype(
        jnp.float32
    )


def bias_block(bias_table, offset, row_count, col_count):
    onehot_map = table_onehot(offset, row_count, col_count, bias_table.shape[1])
    diagonal_vals = jnp.dot(bias_table, onehot_map.T, precision=lax.Precision.HIGHEST)
    return (band_matrix(diagonal_vals, row_count, col_count), onehot_map)


def band_stack(rows, block_count, span_segs):
    segmented = rows.reshape(-1, SEG_LEN, rows.shape[1])
    pieces = [segmented[start : start + block_count] for start in range(span_segs)]
    return jnp.stack(pieces, axis=1).reshape(block_count, span_segs * SEG_LEN, rows.shape[1])


def band_terms(queries, grads_out, log_rows, dot_rows, keys, values, bias_vals, allowed):
    block_count, query_count, feature_count = queries.shape
    key_count = keys.shape[1]
    head_count = log_rows.shape[2]
    query_heads = queries.reshape(block_count, query_count, head_count, -1)
    grad_heads = grads_out.reshape(block_count, query_count, head_count, -1)
    key_heads = keys.reshape(block_count, key_count, head_count, -1)
    value_heads = values.reshape(block_count, key_count, head_count, -1)
    inv_root = query_heads.shape[3] ** (-0.5)
    raw_scores = jnp.einsum(
        "bqhd,bkhd->bhqk", query_heads, key_heads, preferred_element_type=jnp.float32
    )
    scores = raw_scores * inv_root + bias_vals[None]
    log_terms = jnp.transpose(log_rows, (0, 2, 1))[:, :, :, None]
    dot_terms = jnp.transpose(dot_rows, (0, 2, 1))[:, :, :, None]
    weights = jnp.exp(scores - log_terms)
    weights = jnp.where(allowed[:, None, None, :], weights, 0.0)
    weight_grads = jnp.einsum(
        "bqhd,bkhd->bhqk", grad_heads, value_heads, preferred_element_type=jnp.float32
    )
    score_grads = weights * (weight_grads - dot_terms)
    return (
        weights.astype(jnp.bfloat16),
        score_grads.astype(jnp.bfloat16),
        score_grads,
        query_heads,
        key_heads,
        grad_heads,
        inv_root,
    )


def local(query_rows, key_rows, value_rows, out_grad, log_totals, out_dot, bias_table):
    row_count = query_rows.shape[0]
    feature_count = query_rows.shape[1]
    head_count = log_totals.shape[1]
    seg_count = row_count // SEG_LEN
    span_segs = LEFT_SEGS + 1
    band_len = span_segs * SEG_LEN
    need_rows = LEFT_SEGS * SEG_LEN
    lag_total = -(-need_rows // row_count)
    skip_rows = lag_total * row_count - need_rows
    first_row = lax.axis_index(SP_TP) * row_count
    earlier = []
    for lag_count in range(lag_total, 0, -1):
        start_row = skip_rows if lag_count == lag_total else 0
        earlier.append(passed_along((key_rows, value_rows), SP_TP, lag_count))
    all_keys = jnp.concatenate([pair[0] for pair in earlier] + [key_rows], axis=0)
    all_values = jnp.concatenate([pair[1] for pair in earlier] + [value_rows], axis=0)
    key_bands = band_stack(all_keys, seg_count, span_segs)
    value_bands = band_stack(all_values, seg_count, span_segs)
    band_pos = (
        jnp.arange(seg_count, dtype=jnp.int32)[:, None] * SEG_LEN
        + jnp.arange(band_len, dtype=jnp.int32)[None, :]
    )
    allowed = first_row - need_rows + band_pos >= 0
    bias_vals, onehot_map = bias_block(bias_table, need_rows, SEG_LEN, band_len)
    weights_b, score_grads_b, score_grads, query_heads, key_heads, grad_heads, inv_root = (
        band_terms(
            query_rows.reshape(seg_count, SEG_LEN, feature_count),
            out_grad.reshape(seg_count, SEG_LEN, feature_count),
            log_totals.reshape(seg_count, SEG_LEN, head_count),
            out_dot.reshape(seg_count, SEG_LEN, head_count),
            key_bands,
            value_bands,
            bias_vals,
            allowed,
        )
    )
    tap_part = jnp.dot(
        diagonal_sums(jnp.sum(score_grads, axis=0)), onehot_map, precision=lax.Precision.HIGHEST
    )
    query_part = jnp.einsum(
        "bhqk,bkhd->bqhd", score_grads_b, key_heads, preferred_element_type=jnp.float32
    )
    grad_query = (query_part * inv_root).reshape(row_count, feature_count).astype(jnp.bfloat16)
    key_band_grad = jnp.einsum(
        "bhqk,bqhd->bkhd", score_grads_b, query_heads, preferred_element_type=jnp.float32
    )
    key_band_grad = (key_band_grad * inv_root).reshape(seg_count, span_segs, SEG_LEN, feature_count)
    value_band_grad = jnp.einsum(
        "bhqk,bqhd->bkhd", weights_b, grad_heads, preferred_element_type=jnp.float32
    )
    value_band_grad = value_band_grad.reshape(seg_count, span_segs, SEG_LEN, feature_count)
    key_all = sum(
        (
            jnp.pad(key_band_grad[:, lag], ((lag, LEFT_SEGS - lag), (0, 0), (0, 0)))
            for lag in range(span_segs)
        )
    ).reshape(-1, feature_count)
    value_all = sum(
        (
            jnp.pad(value_band_grad[:, lag], ((lag, LEFT_SEGS - lag), (0, 0), (0, 0)))
            for lag in range(span_segs)
        )
    ).reshape(-1, feature_count)
    key_total = key_all[need_rows:]
    value_total = value_all[need_rows:]
    for lag_count in range(1, lag_total + 1):
        lower_row = max(need_rows - lag_count * row_count, 0)
        upper_row = need_rows - (lag_count - 1) * row_count
        returned = passed_along(
            (key_all[lower_row:upper_row], value_all[lower_row:upper_row]), SP_TP, -lag_count
        )
        lead_rows = row_count - (upper_row - lower_row)
        key_total = key_total + returned[0]
        value_total = value_total + returned[1]
    grad_table = over_axes(tap_part, SP_TP)
    return (
        grad_query,
        key_total.astype(jnp.bfloat16),
        value_total.astype(jnp.bfloat16),
        grad_table,
    )


def solution(mesh):
    torus = Mesh(mesh.devices.reshape(12, 8, 2, mesh.shape["tp"]), ("sp_0", "sp_1", "sp_2", "tp"))
    return jax.shard_map(
        local,
        mesh=torus,
        in_specs=(
            P(SP_TP, None),
            P(SP_TP, None),
            P(SP_TP, None),
            P(SP_TP, None),
            P(SP_TP, None),
            P(SP_TP, None),
            P(),
        ),
        out_specs=(P(SP_TP, None), P(SP_TP, None), P(SP_TP, None), P()),
        check_vma=False,
    )
```

profile of v0, /device:TPU:1, one launch (start us, length us, event | category | flops | bytes accessed | tf_op | source)
XLA Modules:
  0.0 276.1 jit_solution(9327182963684908022)
XLA Ops:
  0.6 3.9 %collective-permute-start.1 = (bf16[256,1024]{1,0:T(8,128)(2,1)}, bf16[256,1024]{1,0:T(8,128)(2,1)}, u32[]{:S(2)}, u32[]{:S(2)}) collective-permute-start(bf16[256,1024]{1,0:T(8,128)(2,1)} %param.8), channel_id=1, source_target_pairs={{0,1},{1,2},{2,3},{3,4},{4,5},{5,6},{6,7},{7,8},{8,9},{9,10},{10,1... | collective-permute-start | bytes 1572872 | tf_op jit(solution)/shard_map/ppermute | solution.py:18
  4.6 4.4 %collective-permute-start = (bf16[256,1024]{1,0:T(8,128)(2,1)}, bf16[256,1024]{1,0:T(8,128)(2,1)}, u32[]{:S(2)}, u32[]{:S(2)}) collective-permute-start(bf16[256,1024]{1,0:T(8,128)(2,1)} %param.8), channel_id=1, source_target_pairs={{0,2},{1,3},{2,4},{3,5},{4,6},{5,7},{6,8},{7,9},{8,10},{9,11},{10,... | collective-permute-start | bytes 1572872 | tf_op jit(solution)/shard_map/ppermute | solution.py:18
  9.0 3.1 %collective-permute-start.3 = (bf16[256,1024]{1,0:T(8,128)(2,1)}, bf16[256,1024]{1,0:T(8,128)(2,1)}, u32[]{:S(2)}, u32[]{:S(2)}) collective-permute-start(bf16[256,1024]{1,0:T(8,128)(2,1)} %param.9), channel_id=1, source_target_pairs={{0,1},{1,2},{2,3},{3,4},{4,5},{5,6},{6,7},{7,8},{8,9},{9,10},{10,1... | collective-permute-start | bytes 1572872 | tf_op jit(solution)/shard_map/ppermute | solution.py:18
  12.1 4.9 %collective-permute-start.2 = (bf16[256,1024]{1,0:T(8,128)(2,1)}, bf16[256,1024]{1,0:T(8,128)(2,1)}, u32[]{:S(2)}, u32[]{:S(2)}) collective-permute-start(bf16[256,1024]{1,0:T(8,128)(2,1)} %param.9), channel_id=1, source_target_pairs={{0,2},{1,3},{2,4},{3,5},{4,6},{5,7},{6,8},{7,9},{8,10},{9,11},{10,... | collective-permute-start | bytes 1572872 | tf_op jit(solution)/shard_map/ppermute | solution.py:18
  20.4 1.9 copy.175
  24.8 17.7 %collective-permute-done.2 = bf16[256,1024]{1,0:T(8,128)(2,1)} collective-permute-done((bf16[256,1024]{1,0:T(8,128)(2,1)}, bf16[256,1024]{1,0:T(8,128)(2,1)}, u32[]{:S(2)}, u32[]{:S(2)}) %collective-permute-start.2) | collective-permute-done | bytes 524320 | tf_op jit(solution)/shard_map/ppermute | solution.py:18
  57.7 5.0 %convolution_bitcast_fusion = f32[4,576,8,128]{3,1,2,0:T(8,128)} fusion(f32[4,8,576,64]{2,3,1,0:T(8,128)S(1)} %fusion.5, f32[4,8,64]{2,1,0:T(8,128)S(1)} %get-tuple-element.49, f32[8,64,576]{2,1,0:T(8,128)S(1)} %slice.268, pred[4,576]{1,0:T(4,128)(4,1)S(1)} %add_compare_fusion, bf16[4,64,8,128]{3,2,1,0:T(8,128)(2,1)S(1)} %bitcast.221), kind=kOutput, calls=%fused_computation.13 | convolution fusion | flops 307888128 | bytes 15870208 | tf_op jit(solution)/shard_map/bhqk,bqhd->bkhd/dot_general | solution.py:146
  62.7 4.2 %fusion.52 = (f32[8,64,576]{2,1,0:T(8,128)S(1)}, bf16[4,8,64,576]{3,2,1,0:T(8,128)(2,1)}) fusion(f32[4,8,64]{2,1,0:T(8,128)S(1)} %get-tuple-element.48, bf16[4,64,8,128]{3,2,1,0:T(8,128)(2,1)S(1)} %bitcast.222, bf16[4,576,8,128]{3,2,1,0:T(8,128)(2,1)S(1)} %bitcast.220, f32[4,8,64]{2,1,0:T(8,128)S(1)} %get-tuple-element.49, f32[8,64,576]{2,1,0:T(8,128)S(1)} %slice.268, ...), kind=kOutput, calls=%fused_computation.101 | convolution fusion | flops 311132160 | bytes 14698752 | tf_op jit(solution)/shard_map/bqhd,bkhd->bhqk/dot_general | solution.py:83
  70.6 12.8 %copy.146 = f32[4,576,8,128]{3,2,1,0:T(8,128)} copy(f32[4,576,8,128]{3,1,2,0:T(8,128)} %convolution_bitcast_fusion) | data formatting | bytes 18874368 | tf_op jit(solution)/shard_map/bhqk,bqhd->bkhd/transpose | solution.py:146
  83.3 11.2 %reshape.119 = f32[4,9,64,1024]{3,2,1,0:T(8,128)} reshape(f32[4,576,8,128]{3,2,1,0:T(8,128)} %copy.146) | data formatting | bytes 18874368 | tf_op jit(solution)/shard_map/reshape | solution.py:149
  94.5 4.7 %slice_bitcast_fusion.8 = (f32[4,64,1024]{2,1,0:T(8,128)S(1)}, f32[4,64,1024]{2,1,0:T(8,128)S(1)}, f32[4,64,1024]{2,1,0:T(8,128)S(1)}, f32[4,64,1024]{2,1,0:T(8,...) fusion(f32[4,9,64,1024]{3,2,1,0:T(8,128)} %reshape.119), kind=kLoop, calls=%fused_computation.37 | loop fusion | bytes 18874368 | tf_op jit(solution)/shard_map/squeeze | solution.py:158
  101.9 13.9 %collective-permute-start.7 = (f32[256,1024]{1,0:T(8,128)}, f32[256,1024]{1,0:T(8,128)}, u32[]{:S(2)}, u32[]{:S(2)}) collective-permute-start(f32[256,1024]{1,0:T(8,128)} %bitcast.67), channel_id=1, source_target_pairs={{2,0},{3,1},{4,2},{5,3},{6,4},{7,5},{8,6},{9,7},{10,8},{11,9},{12,... | collective-permute-start | bytes 3145736 | tf_op jit(solution)/shard_map/ppermute | solution.py:18
  115.7 2.1 collective-permute-start.6
  119.4 9.1 %copy.136 = f32[4,576,8,128]{3,2,1,0:T(8,128)} copy(f32[4,576,8,128]{3,1,2,0:T(8,128)S(1)} %multiply_bitcast_fusion) | data formatting | bytes 18874368 | tf_op jit(solution)/shard_map/mul | solution.py:145
  128.5 11.1 %reshape.118 = f32[4,9,64,1024]{3,2,1,0:T(8,128)} reshape(f32[4,576,8,128]{3,2,1,0:T(8,128)} %copy.136) | data formatting | bytes 18874368 | tf_op jit(solution)/shard_map/reshape | solution.py:145
  139.6 4.7 %slice_bitcast_fusion.17 = (f32[4,64,1024]{2,1,0:T(8,128)S(1)}, f32[4,64,1024]{2,1,0:T(8,128)S(1)}, f32[4,64,1024]{2,1,0:T(8,128)S(1)}, f32[4,64,1024]{2,1,0:T(8...) fusion(f32[4,9,64,1024]{3,2,1,0:T(8,128)} %reshape.118), kind=kLoop, calls=%fused_computation.46 | loop fusion | bytes 18874368 | tf_op jit(solution)/shard_map/squeeze | solution.py:152
  147.1 2.0 collective-permute-start.5
  149.1 2.5 collective-permute-start.4
  154.6 48.1 %psum.28 = f32[8,320]{1,0:T(8,128)S(1)} all-reduce(f32[8,320]{1,0:T(8,128)S(1)} %fusion.37), channel_id=1, replica_groups=mesh['sp_0'=12,'sp_1'=8,'sp_2'=2,'tp'=4] {'sp_0'}, use_global_device_ids=true, to_apply=%region_2.3 | all-reduce | flops 2560 | bytes 20480 | tf_op jit(solution)/shard_map/psum | solution.py:22
  202.7 21.0 %psum.29 = f32[8,320]{1,0:T(8,128)S(1)} all-reduce(f32[8,320]{1,0:T(8,128)S(1)} %psum.28), channel_id=1, replica_groups=mesh['sp_0'=12,'sp_1'=8,'sp_2'=2,'tp'=4] {'sp_1'}, use_global_device_ids=true, to_apply=%region_3.4 | all-reduce | flops 2560 | bytes 20480 | tf_op jit(solution)/shard_map/psum | solution.py:22
  223.8 35.8 %psum.30 = f32[8,320]{1,0:T(8,128)S(1)} all-reduce(f32[8,320]{1,0:T(8,128)S(1)} %psum.29), channel_id=1, replica_groups=mesh['sp_0'=12,'sp_1'=8,'sp_2'=2,'tp'=4] {'sp_2'}, use_global_device_ids=true, to_apply=%region_4.5 | all-reduce | flops 2560 | bytes 20480 | tf_op jit(solution)/shard_map/psum | solution.py:22
  259.5 11.7 %psum.31 = f32[8,320]{1,0:T(8,128)} all-reduce(f32[8,320]{1,0:T(8,128)S(1)} %psum.30), channel_id=1, replica_groups=mesh['sp_0'=12,'sp_1'=8,'sp_2'=2,'tp'=4] {'tp'}, use_global_device_ids=true, to_apply=%region_5.6 | all-reduce | flops 2560 | bytes 20480 | tf_op jit(solution)/shard_map/psum | solution.py:22
  271.2 2.6 fusion.34
  273.8 2.3 fusion.36
  (86 shorter events, 34.2 us)
Async XLA Ops:
  0.6 16.4 %copy-start = (f32[8,320]{1,0:T(8,128)S(1)}, f32[8,320]{1,0:T(8,128)}, u32[]{:S(2)}) copy-start(f32[8,320]{1,0:T(8,128)} %param.13) | copy-start | bytes 30724
  0.6 45.7 %collective-permute-start.1 = (bf16[256,1024]{1,0:T(8,128)(2,1)}, bf16[256,1024]{1,0:T(8,128)(2,1)}, u32[]{:S(2)}, u32[]{:S(2)}) collective-permute-start(bf16[256,1024]{1,0:T(8,128)(2,1)} %param.8), channel_id=1, source_target_pairs={{0,1},{1,2},{2,3},{3,4},{4,5},{5,6},{6,7},{7,8},{8,9},{9,10},{10,1... | collective-permute-start | bytes 1572872 | tf_op jit(solution)/shard_map/ppermute | solution.py:18
  4.6 38.9 %collective-permute-start = (bf16[256,1024]{1,0:T(8,128)(2,1)}, bf16[256,1024]{1,0:T(8,128)(2,1)}, u32[]{:S(2)}, u32[]{:S(2)}) collective-permute-start(bf16[256,1024]{1,0:T(8,128)(2,1)} %param.8), channel_id=1, source_target_pairs={{0,2},{1,3},{2,4},{3,5},{4,6},{5,7},{6,8},{7,9},{8,10},{9,11},{10,... | collective-permute-start | bytes 1572872 | tf_op jit(solution)/shard_map/ppermute | solution.py:18
  9.0 35.7 %collective-permute-start.3 = (bf16[256,1024]{1,0:T(8,128)(2,1)}, bf16[256,1024]{1,0:T(8,128)(2,1)}, u32[]{:S(2)}, u32[]{:S(2)}) collective-permute-start(bf16[256,1024]{1,0:T(8,128)(2,1)} %param.9), channel_id=1, source_target_pairs={{0,1},{1,2},{2,3},{3,4},{4,5},{5,6},{6,7},{7,8},{8,9},{9,10},{10,1... | collective-permute-start | bytes 1572872 | tf_op jit(solution)/shard_map/ppermute | solution.py:18
  12.1 30.4 %collective-permute-start.2 = (bf16[256,1024]{1,0:T(8,128)(2,1)}, bf16[256,1024]{1,0:T(8,128)(2,1)}, u32[]{:S(2)}, u32[]{:S(2)}) collective-permute-start(bf16[256,1024]{1,0:T(8,128)(2,1)} %param.9), channel_id=1, source_target_pairs={{0,2},{1,3},{2,4},{3,5},{4,6},{5,7},{6,8},{7,9},{8,10},{9,11},{10,... | collective-permute-start | bytes 1572872 | tf_op jit(solution)/shard_map/ppermute | solution.py:18
  24.4 21.5 %copy-start.6 = (bf16[256,1024]{1,0:T(8,128)(2,1)S(1)}, bf16[256,1024]{1,0:T(8,128)(2,1)}, u32[]{:S(2)}) copy-start(bf16[256,1024]{1,0:T(8,128)(2,1)} %param.9) | copy-start | bytes 1572868
  45.8 1.7 copy-start.7
  55.4 2.2 copy-start.2
  55.5 2.2 copy-start.5
  100.2 17.7 %copy-start.3 = (bf16[4,8,64,576]{3,2,1,0:T(8,128)(2,1)S(1)}, bf16[4,8,64,576]{3,2,1,0:T(8,128)(2,1)}, u32[]{:S(2)}) copy-start(bf16[4,8,64,576]{3,2,1,0:T(8,128)(2,1)} %get-tuple-element.45) | copy-start | bytes 7077892
  101.9 169.3 %collective-permute-start.7 = (f32[256,1024]{1,0:T(8,128)}, f32[256,1024]{1,0:T(8,128)}, u32[]{:S(2)}, u32[]{:S(2)}) collective-permute-start(f32[256,1024]{1,0:T(8,128)} %bitcast.67), channel_id=1, source_target_pairs={{2,0},{3,1},{4,2},{5,3},{6,4},{7,5},{8,6},{9,7},{10,8},{11,9},{12,... | collective-permute-start | bytes 3145736 | tf_op jit(solution)/shard_map/ppermute | solution.py:18
  115.7 155.5 %collective-permute-start.6 = (f32[256,1024]{1,0:T(8,128)}, f32[256,1024]{1,0:T(8,128)}, u32[]{:S(2)}, u32[]{:S(2)}) collective-permute-start(f32[256,1024]{1,0:T(8,128)} %bitcast.66), channel_id=1, source_target_pairs={{1,0},{2,1},{3,2},{4,3},{5,4},{6,5},{7,6},{8,7},{9,8},{10,9},{11,1... | collective-permute-start | bytes 3145736 | tf_op jit(solution)/shard_map/ppermute | solution.py:18
  139.6 12.0 %slice-start = ((s8[4718592]{0:T(1024)(128)(4,1)}), s8[524288]{0:T(1024)(128)(4,1)S(1)}, s32[]{:S(2)}) async-start(s8[4718592]{0:T(1024)(128)(4,1)} %bitcast.210), calls=%async_computation | async-start | bytes 1048576
  144.4 7.2 %slice-start.1 = ((s8[4718592]{0:T(1024)(128)(4,1)}), s8[4194304]{0:T(1024)(128)(4,1)S(1)}, s32[]{:S(2)}) async-start(s8[4718592]{0:T(1024)(128)(4,1)} %bitcast.210), calls=%async_computation.1 | async-start | bytes 8388608
  145.4 6.2 %copy-start.4 = (bf16[4,8,64,576]{3,2,1,0:T(8,128)(2,1)S(1)}, bf16[4,8,64,576]{3,2,1,0:T(8,128)(2,1)}, u32[]{:S(2)}) copy-start(bf16[4,8,64,576]{3,2,1,0:T(8,128)(2,1)} %get-tuple-element.45) | copy-start | bytes 7077892
  147.1 126.7 %collective-permute-start.5 = (f32[256,1024]{1,0:T(8,128)}, f32[256,1024]{1,0:T(8,128)S(1)}, u32[]{:S(2)}, u32[]{:S(2)}) collective-permute-start(f32[256,1024]{1,0:T(8,128)} %bitcast.54), channel_id=1, source_target_pairs={{2,0},{3,1},{4,2},{5,3},{6,4},{7,5},{8,6},{9,7},{10,8},{11,9},{12,... | collective-permute-start | bytes 3145736 | tf_op jit(solution)/shard_map/ppermute | solution.py:18
  149.1 124.6 %collective-permute-start.4 = (f32[256,1024]{1,0:T(8,128)}, f32[256,1024]{1,0:T(8,128)}, u32[]{:S(2)}, u32[]{:S(2)}) collective-permute-start(f32[256,1024]{1,0:T(8,128)} %bitcast.53), channel_id=1, source_target_pairs={{1,0},{2,1},{3,2},{4,3},{5,4},{6,5},{7,6},{8,7},{9,8},{10,9},{11,1... | collective-permute-start | bytes 3145736 | tf_op jit(solution)/shard_map/ppermute | solution.py:18
  151.6 124.4 %copy-start.1 = (f32[8,320]{1,0:T(8,128)S(1)}, f32[8,320]{1,0:T(8,128)}, u32[]{:S(2)}) copy-start(f32[8,320]{1,0:T(8,128)} %param.13) | copy-start | bytes 30724
where the time goes:
time: 279 us; the launch traced here: 276 us
  blocking collectives  117 us (42%)
  local copies, waits for them, and re-layouts  82 us (29%)
  starting transfers between devices  36.8 us (13%)
  waiting for transfers between devices  17.7 us (6%)
  matrix products  14.8 us (5%)
  other arithmetic  7.03 us (3%)
    psum x4, blocking collectives, over_axes(): return functools.reduce(lax.psum, axes, shard)  117 us
    ppermute x8, starting transfers between devices, passed_along(): return lax.ppermute(block, axis, route)  36.8 us
    unnamed x52, local copies, waits for them, and re-layouts  19.8 us
    ppermute x8, waiting for transfers between devices, passed_along(): return lax.ppermute(block, axis, route)  17.7 us
    transpose x1, local copies, waits for them, and re-layouts, local(): jnp.einsum('bhqk,bqhd->bkhd', weights_b, grad_heads, preferred_element_ty...  12.8 us
    reshape x1, local copies, waits for them, and re-layouts, local(): value_band_grad.reshape(seg_count, span_segs, SEG_LEN, feature_count)  11.2 us
    reshape x1, local copies, waits for them, and re-layouts, local(): (key_band_grad * inv_root).reshape(seg_count, span_segs, SEG_LEN, feature...  11.1 us
    mul x1, local copies, waits for them, and re-layouts, local(): key_band_grad * inv_root  9.12 us
  transfers between devices with their start and end apart: 8, of which 1 were waited for; matrix products, arithmetic and copies ran while one was open for 17% of the time, Pallas kernels for 0%

commit v1 on v0

v1 whole, which is shorter than its diff:
```python
import functools
import math

import jax
import jax.numpy as jnp
from jax import lax
from jax.experimental import pallas as pl
from jax.experimental.pallas import tpu as pltpu
from jax.sharding import PartitionSpec as P

SEG_LEN = 64
REL_CLIP = 256
ROWS = 256
HALF = 128
BAND = 640
HEADS = 8
HEAD_DIM = 128
TABLE_LEN = 320
LOG2E = math.log2(math.e)
FAR = 1e30
MESH = pl.DeviceIdType.MESH
F32 = jnp.float32
BF16 = jnp.bfloat16


def dot_nt(lhs, rhs):
    return lax.dot_general(lhs, rhs, (((1,), (1,)), ((), ())), preferred_element_type=F32)


def dot_nn(lhs, rhs):
    return lax.dot_general(lhs, rhs, (((1,), (0,)), ((), ())), preferred_element_type=F32)


def dot_tn(lhs, rhs):
    return lax.dot_general(lhs, rhs, (((0,), (0,)), ((), ())), preferred_element_type=F32)


def kernel(
    sp_size,
    tp_size,
    q_hbm,
    k_hbm,
    v_hbm,
    g_hbm,
    lse_hbm,
    dot_hbm,
    table_ref,
    dq_hbm,
    dk_hbm,
    dv_hbm,
    gt_ref,
    kv,
    qg,
    stats,
    wide,
    bias,
    ext,
    acc,
    outs,
    load_sem,
    stat_sem,
    out_sem,
    kv_send,
    kv_recv,
    qg_send,
    qg_recv,
    st_send,
    st_recv,
):
    sp, tp = lax.axis_index("sp"), lax.axis_index("tp")
    last_tp, first_tp = tp == tp_size - 1, tp == 0
    nxt = (
        lax.rem(sp + jnp.where(last_tp, 1, 0), sp_size),
        lax.rem(tp + 1, tp_size),
    )
    prv = (
        lax.rem(sp + sp_size - jnp.where(first_tp, 1, 0), sp_size),
        lax.rem(tp + tp_size - 1, tp_size),
    )
    me = sp * tp_size + tp
    total = sp_size * tp_size
    inv_root = HEAD_DIM**-0.5

    def loads(k):
        ahead, back = k, HEADS - 1 - k
        places = [
            (k_hbm, kv.at[ahead, 0, pl.ds(512, ROWS)], ahead),
            (v_hbm, kv.at[ahead, 1, pl.ds(512, ROWS)], ahead),
            (q_hbm, qg.at[back, 0, pl.ds(0, ROWS)], back),
            (g_hbm, qg.at[back, 1, pl.ds(0, ROWS)], back),
        ]
        return [
            pltpu.make_async_copy(
                src.at[:, pl.ds(pl.multiple_of(h * HEAD_DIM, HEAD_DIM), HEAD_DIM)],
                dst,
                load_sem.at[n, h],
            )
            for n, (src, dst, h) in enumerate(places)
        ]

    def stores(k):
        ahead, back = k, HEADS - 1 - k
        return [
            pltpu.make_async_copy(
                outs.at[n, h],
                out.at[:, pl.ds(pl.multiple_of(h * HEAD_DIM, HEAD_DIM), HEAD_DIM)],
                out_sem.at[n, h],
            )
            for n, (out, h) in enumerate(((dq_hbm, ahead), (dk_hbm, back), (dv_hbm, back)))
        ]

    def kv_copy(h, lag):
        src, dst = (512, 256) if lag == 0 else (256, 0)
        return pltpu.make_async_remote_copy(
            src_ref=kv.at[h, :, pl.ds(src, ROWS)],
            dst_ref=kv.at[h, :, pl.ds(dst, ROWS)],
            send_sem=kv_send.at[lag, h],
            recv_sem=kv_recv.at[lag, h],
            device_id=nxt,
            device_id_type=MESH,
        )

    def qg_copy(h, lag):
        return pltpu.make_async_remote_copy(
            src_ref=qg.at[h, :, pl.ds(lag * ROWS, ROWS)],
            dst_ref=qg.at[h, :, pl.ds((lag + 1) * ROWS, ROWS)],
            send_sem=qg_send.at[lag, h],
            recv_sem=qg_recv.at[lag, h],
            device_id=prv,
            device_id_type=MESH,
        )

    def st_copy(lag):
        return pltpu.make_async_remote_copy(
            src_ref=stats.at[lag],
            dst_ref=stats.at[lag + 1],
            send_sem=st_send.at[lag],
            recv_sem=st_recv.at[lag],
            device_id=prv,
            device_id_type=MESH,
        )

    stat_loads = [
        pltpu.make_async_copy(lse_hbm, stats.at[0, pl.ds(0, HEADS)], stat_sem.at[0]),
        pltpu.make_async_copy(dot_hbm, stats.at[0, pl.ds(HEADS, HEADS)], stat_sem.at[1]),
    ]

    barrier = pltpu.get_barrier_semaphore()
    for neighbour in (nxt, prv):
        pl.semaphore_signal(barrier, inc=1, device_id=neighbour, device_id_type=MESH)

    for copy in stat_loads:
        copy.start()

    @pl.loop(0, HEADS)
    def _(k):
        for copy in loads(k):
            copy.start()

    pl.semaphore_wait(barrier, 2)

    def await_loads(k):
        for copy in loads(k):
            copy.wait()

    def send_own(k):
        kv_copy(k, 0).start()
        qg_copy(HEADS - 1 - k, 0).start()

    for copy in stat_loads:
        copy.wait()
    st_copy(0).start()
    for k in range(2):
        await_loads(k)
        send_own(k)
    pl.loop(2, HEADS)(await_loads)

    ext[...] = jnp.broadcast_to(table_ref[:, TABLE_LEN - 1 : TABLE_LEN], (HEADS, 512))
    ext[:, 0:TABLE_LEN] = table_ref[...]
    ext[...] = pltpu.roll(ext[...], 65, 1) * LOG2E
    key_row = lax.broadcasted_iota(jnp.int32, (HALF, HALF), 0)
    query_col = lax.broadcasted_iota(jnp.int32, (HALF, HALF), 1)
    near_off = (key_row >= SEG_LEN) & (query_col < SEG_LEN)
    far_off = (key_row < SEG_LEN) & (query_col >= SEG_LEN)

    @pl.loop(0, HEADS)
    def _(h):
        row = ext[pl.ds(h, 1), :]
        for d in range(3):
            low = row[:, HALF * d : HALF * (d + 1)]
            high = row[:, HALF * (d + 1) : HALF * (d + 2)]
            around = jnp.broadcast_to(jnp.concatenate([high, low], axis=1), (HALF, 2 * HALF))
            tile = pltpu.roll(around, 0, 1, stride=1, stride_axis=0)[:, :HALF]
            if d == 0:
                tile = jnp.where(near_off, -FAR, tile)
            bias[h, d] = tile
        flat = jnp.broadcast_to(row[:, 511:512], (HALF, HALF))
        bias[h, 3] = flat
        bias[h, 4] = jnp.where(far_off, -FAR, flat)

    st_copy(0).wait_recv()
    st_copy(1).start()
    st_copy(1).wait_recv()

    def off(cond):
        return jnp.where(cond, FAR, 0.0).astype(F32)

    key_off = [off(me < 0), off(me < 1), off(me < 2)]
    query_off = [off(me < 0), off(me + 1 >= total), off(me + 2 >= total)]
    for lag in range(3):
        for n in range(2 * HEADS):
            row = stats[lag, n : n + 1, :]
            if n < HEADS:
                row = row * LOG2E + query_off[lag]
            wide[lag, n] = jnp.broadcast_to(row, (8, ROWS))

    def tile_terms(scores, weight_grads, bias_tile, log_row, dot_row):
        weights = jnp.exp2(scores * (inv_root * LOG2E) + (bias_tile - log_row))
        return weights, weights * (weight_grads - dot_row)

    def add_to(side, part, d, score_grads):
        if part == 0:
            acc[side, d] = score_grads
        else:
            acc[side, d] += score_grads

    def query_side(h):
        for part in range(2):
            rows = pl.ds(part * HALF, HALF)
            queries, grads = qg[h, 0, rows, :], qg[h, 1, rows, :]
            keys = kv[h, 0, pl.ds(part * HALF, BAND), :]
            values = kv[h, 1, pl.ds(part * HALF, BAND), :]
            scores = dot_nt(keys, queries)
            weight_grads = dot_nt(values, grads)
            log_row = wide[0, h, 0:1, rows]
            dot_row = wide[0, HEADS + h, 0:1, rows]
            pieces = []
            for t in range(5):
                d, lag = 4 - t, 2 - (part + t) // 2
                cut = slice(t * HALF, (t + 1) * HALF)
                _, score_grads = tile_terms(
                    scores[cut], weight_grads[cut], bias[h, d], log_row + key_off[lag], dot_row
                )
                add_to(0, part, d, score_grads)
                pieces.append(score_grads.astype(BF16))
            total_grads = dot_tn(jnp.concatenate(pieces, axis=0), keys)
            outs[0, h, rows, :] = (total_grads * inv_root).astype(BF16)

    def key_side(h):
        for part in range(2):
            rows = pl.ds(part * HALF, HALF)
            own = pl.ds(512 + part * HALF, HALF)
            keys, values = kv[h, 0, own, :], kv[h, 1, own, :]
            queries = qg[h, 0, pl.ds(part * HALF, BAND), :]
            grads = qg[h, 1, pl.ds(part * HALF, BAND), :]
            scores = dot_nt(keys, queries)
            weight_grads = dot_nt(values, grads)
            score_pieces, weight_pieces = [], []
            for d in range(5):
                lag, cols = (part + d) // 2, pl.ds((part + d) % 2 * HALF, HALF)
                cut = slice(d * HALF, (d + 1) * HALF)
                log_row = wide[lag, h, 0:1, cols]
                dot_row = wide[lag, HEADS + h, 0:1, cols]
                weights, score_grads = tile_terms(
                    scores[:, cut], weight_grads[:, cut], bias[h, d], log_row, dot_row
                )
                add_to(1, part, d, score_grads)
                score_pieces.append(score_grads.astype(BF16))
                weight_pieces.append(weights.astype(BF16))
            key_grads = dot_nn(jnp.concatenate(score_pieces, axis=1), queries)
            outs[1, h, rows, :] = (key_grads * inv_root).astype(BF16)
            value_grads = dot_nn(jnp.concatenate(weight_pieces, axis=1), grads)
            outs[2, h, rows, :] = value_grads.astype(BF16)

    def table_row(side, h):
        zeros = jnp.zeros((HALF, HALF), F32)
        part = jnp.concatenate([acc[side, 0], acc[side, 1], acc[side, 2], zeros], axis=1)
        for step in (64, 32, 16, 8):
            part = part[:step] + pltpu.roll(part[step:], 512 - step, 1)
        row_id = lax.broadcasted_iota(jnp.int32, (8, 512), 0)
        for step in (4, 2, 1):
            moved = pltpu.roll(part, 512 - step, 1)
            part = jnp.where((row_id & step) != 0, moved, part)
        far = jnp.sum(acc[side, 3] + acc[side, 4], keepdims=True)
        by_distance = pltpu.roll(jnp.sum(part, axis=0, keepdims=True), SEG_LEN - 1, 1)
        lane = lax.broadcasted_iota(jnp.int32, (1, 512), 1)
        top = TABLE_LEN - 1
        clipped = (lane >= top) & (lane < 448)
        far = far + jnp.sum(jnp.where(clipped, by_distance, 0.0), keepdims=True)
        row = jnp.where(lane < top, by_distance, jnp.where(lane == top, far, 0.0))
        gt_ref[pl.ds(h, 1), :] = row

    @pl.loop(0, HEADS + 1)
    def _(k):
        @pl.when(k < HEADS)
        def _():
            kv_copy(k, 0).wait_recv()
            kv_copy(k, 1).start()
            qg_copy(HEADS - 1 - k, 0).wait_recv()
            qg_copy(HEADS - 1 - k, 1).start()

        @pl.when(k < HEADS - 2)
        def _():
            send_own(k + 2)

        @pl.when(k >= 1)
        def _():
            ahead, back = k - 1, HEADS - k
            kv_copy(ahead, 1).wait_recv()
            query_side(ahead)
            qg_copy(back, 1).wait_recv()
            key_side(back)

            @pl.when(k <= HEADS // 2)
            def _():
                table_row(0, ahead)
                table_row(1, back)

            for copy in stores(ahead):
                copy.start()

    @pl.loop(0, HEADS)
    def _(h):
        for lag in range(2):
            kv_copy(h, lag).wait_send()
            qg_copy(h, lag).wait_send()
        for copy in stores(h):
            copy.wait()

    st_copy(0).wait_send()
    st_copy(1).wait_send()


def solution(mesh):
    sp_size, tp_size = mesh.shape["sp"], mesh.shape["tp"]

    def local(query_rows, key_rows, value_rows, out_grad, log_totals, out_dot, bias_table):
        hbm = pl.BlockSpec(memory_space=pl.ANY)
        vmem = pl.BlockSpec(memory_space=pltpu.VMEM)
        rows = jax.ShapeDtypeStruct(query_rows.shape, BF16)
        grad_query, grad_key, grad_value, table_part = pl.pallas_call(
            functools.partial(kernel, sp_size, tp_size),
            out_shape=(rows, rows, rows, jax.ShapeDtypeStruct((HEADS, 512), F32)),
            in_specs=[hbm] * 6 + [vmem],
            out_specs=(hbm, hbm, hbm, vmem),
            scratch_shapes=[
                pltpu.VMEM((HEADS, 2, 3 * ROWS, HEAD_DIM), BF16),
                pltpu.VMEM((HEADS, 2, 3 * ROWS, HEAD_DIM), BF16),
                pltpu.VMEM((3, 2 * HEADS, ROWS), F32),
                pltpu.VMEM((3, 2 * HEADS, 8, ROWS), F32),
                pltpu.VMEM((HEADS, 5, HALF, HALF), F32),
                pltpu.VMEM((HEADS, 512), F32),
                pltpu.VMEM((2, 5, HALF, HALF), F32),
                pltpu.VMEM((3, HEADS, ROWS, HEAD_DIM), BF16),
                pltpu.SemaphoreType.DMA((4, HEADS)),
                pltpu.SemaphoreType.DMA((2,)),
                pltpu.SemaphoreType.DMA((3, HEADS)),
                pltpu.SemaphoreType.DMA((2, HEADS)),
                pltpu.SemaphoreType.DMA((2, HEADS)),
                pltpu.SemaphoreType.DMA((2, HEADS)),
                pltpu.SemaphoreType.DMA((2, HEADS)),
                pltpu.SemaphoreType.DMA((2,)),
                pltpu.SemaphoreType.DMA((2,)),
            ],
            compiler_params=pltpu.CompilerParams(
                collective_id=0, has_side_effects=True
            ),
        )(query_rows, key_rows, value_rows, out_grad, log_totals.T, out_dot.T, bias_table)
        grad_table = lax.psum(table_part[:, :TABLE_LEN], ("sp", "tp"))
        return grad_query, grad_key, grad_value, grad_table

    split = P(("sp", "tp"), None)
    return jax.shard_map(
        local,
        mesh=mesh,
        in_specs=(split,) * 6 + (P(),),
        out_specs=(split, split, split, P()),
        check_vma=False,
    )
```

time: 279 us -> 183 us (0.66)
  local copies, waits for them, and re-layouts: 82 us -> 4.66 us
  Pallas kernels: 0 us -> 64.5 us
  starting transfers between devices: 36.8 us -> 0 us
  waiting for transfers between devices: 17.7 us -> 0 us
  matrix products: 14.8 us -> 0 us
  other arithmetic: 7.03 us -> 0 us
  blocking collectives: 117 us -> 113 us
    pallas_call x0 -> x1, Pallas kernels: none -> 64.5 us  [local(): pl.pallas_call(functools.partial(kernel, sp_size, tp_size), out_shape=(ro...]
    ppermute x8 -> x0, starting transfers between devices: 36.8 us -> none  [passed_along(): return lax.ppermute(block, axis, route)]
    reshape x6 -> x0, local copies, waits for them, and re-layouts: 25.9 us -> none  [the longest x1 11.2 us: local(): value_band_grad.reshape(seg_count, span_segs, SEG_LEN, feature_count)]
    ppermute x8 -> x0, waiting for transfers between devices: 17.7 us -> none  [passed_along(): return lax.ppermute(block, axis, route)]
    unnamed x52 -> x7, local copies, waits for them, and re-layouts: 19.8 us -> 3.95 us
    dot_general x7 -> x0, matrix products: 14.8 us -> none  [the longest x1 5 us: local(): jnp.einsum('bhqk,bqhd->bkhd', weights_b, grad_heads, preferred_element_ty...]
    transpose x2 -> x0, local copies, waits for them, and re-layouts: 12.8 us -> none  [the longest x1 12.8 us: local(): jnp.einsum('bhqk,bqhd->bkhd', weights_b, grad_heads, preferred_element_ty...]
    squeeze x2 -> x0, local copies, waits for them, and re-layouts: 9.43 us -> none  [the longest x1 4.74 us: local(): key_band_grad[:, lag]]
  transfers between devices with their start and end apart: 8 -> 0, of which waited for: 1 -> 0; matrix products, arithmetic and copies ran while one was open for 17% -> 0% of each run, Pallas kernels for 0% -> 0%
where the time goes in v1:
time: 183 us; the launch traced here: 182 us
  blocking collectives  113 us (62%)
  Pallas kernels  64.5 us (35%)
  local copies, waits for them, and re-layouts  4.66 us (3%)
    psum x1, blocking collectives, local(): grad_table = lax.psum(table_part[:, :TABLE_LEN], ('sp', 'tp'))  113 us
    pallas_call x1, Pallas kernels, local(): pl.pallas_call(functools.partial(kernel, sp_size, tp_size), out_shape=(ro...  64.5 us
    unnamed x7, local copies, waits for them, and re-layouts  3.95 us

profile of v1, /device:TPU:1, one launch (start us, length us, event | category | flops | bytes accessed | tf_op | source)
XLA Modules:
  0.0 182.4 jit_solution(4905967633394025964)
XLA Ops:
  0.6 64.5 %shard_map.102 = (bf16[256,1024]{1,0:T(8,128)(2,1)}, bf16[256,1024]{1,0:T(8,128)(2,1)}, bf16[256,1024]{1,0:T(8,128)(2,1)}, f32[8,512]{1,0:T(8,128)}) custom-call(bf16[256,1024]{1,0:T(8,128)(2,1)} %q_hbm.1, bf16[256,1024]{1,0:T(8,128)(2,1)} %k_hbm.1, bf16[256,1024]{1,0:T(8,128)(2,1)} %v_hbm.1, bf16[256,1024]{1,0:T(8,128)(2,1)} %g_hbm.1, f32[8,256]{1,0:T(8,128)} %bitcast.2, ...), custom_call_target="tpu_custom_call" | custom-call | tf_op jit(solution)/shard_map/pallas_call | solution.py:341
  65.2 0.7 slice.3
  65.9 112.6 %psum.7 = f32[8,320]{1,0:T(8,128)} all-reduce(f32[8,320]{1,0:T(8,128)S(1)} %slice.3), channel_id=1, replica_groups=mesh['sp'=192,'tp'=4] {'sp','tp'}, use_global_device_ids=true, to_apply=%region_0.0 | all-reduce | flops 2560 | bytes 20480 | tf_op jit(solution)/shard_map/psum | solution.py:369
  178.5 0.0 copy-start.1
  178.5 1.9 %copy.14 = bf16[256,1024]{1,0:T(8,128)(2,1)} copy(bf16[256,1024]{1,0:T(8,128)(2,1)} %get-tuple-element.16) | data formatting | bytes 1048576
  180.4 0.0 copy-done.1
  180.4 0.0 copy-start
  180.4 0.8 copy.15
  181.2 0.4 copy-done
  181.6 0.8 copy.16
Async XLA Ops:
  178.5 1.9 %copy-start.1 = (bf16[256,1024]{1,0:T(8,128)(2,1)S(1)}, bf16[256,1024]{1,0:T(8,128)(2,1)}, u32[]{:S(2)}) copy-start(bf16[256,1024]{1,0:T(8,128)(2,1)} %get-tuple-element.17) | copy-start | bytes 1572868
  180.4 1.2 copy-start

commit v2 on v1

--- a/solution.py
+++ b/solution.py
@@ -18,6 +18,8 @@
 TABLE_LEN = 320
 LOG2E = math.log2(math.e)
 FAR = 1e30
+SP_SHAPE = (12, 8, 2)
+GROUP = HEADS // 2
 MESH = pl.DeviceIdType.MESH
 F32 = jnp.float32
 BF16 = jnp.bfloat16
@@ -45,9 +47,9 @@
     lse_hbm,
     dot_hbm,
     table_ref,
-    dq_hbm,
-    dk_hbm,
-    dv_hbm,
+    dq_ref,
+    dk_ref,
+    dv_ref,
     gt_ref,
     kv,
     qg,
@@ -56,10 +58,23 @@
     bias,
     ext,
     acc,
-    outs,
+    tab,
+    tab_core,
+    tab_y,
+    tab_z,
+    tab_x,
+    tab_all,
     load_sem,
     stat_sem,
-    out_sem,
+    core_sem,
+    y_send,
+    y_recv,
+    z_send,
+    z_recv,
+    x_send,
+    x_recv,
+    all_send,
+    all_recv,
     kv_send,
     kv_recv,
     qg_send,
@@ -77,9 +92,18 @@
         lax.rem(sp + sp_size - jnp.where(first_tp, 1, 0), sp_size),
         lax.rem(tp + tp_size - 1, tp_size),
     )
+    z_size, y_size, core_size = SP_SHAPE
+    at_z, at_y, at_core = sp // (y_size * core_size), sp // core_size % y_size, sp % core_size
+
+    def at(z, y, core):
+        return ((z * y_size + y) * core_size + core, tp)
+
     me = sp * tp_size + tp
     total = sp_size * tp_size
     inv_root = HEAD_DIM**-0.5
+
+    def cols_of(h):
+        return pl.ds(pl.multiple_of(h * HEAD_DIM, HEAD_DIM), HEAD_DIM)
 
     def loads(k):
         ahead, back = k, HEADS - 1 - k
@@ -91,22 +115,11 @@
         ]
         return [
             pltpu.make_async_copy(
-                src.at[:, pl.ds(pl.multiple_of(h * HEAD_DIM, HEAD_DIM), HEAD_DIM)],
+                src.at[:, cols_of(h)],
                 dst,
                 load_sem.at[n, h],
             )
             for n, (src, dst, h) in enumerate(places)
-        ]
-
-    def stores(k):
-        ahead, back = k, HEADS - 1 - k
-        return [
-            pltpu.make_async_copy(
-                outs.at[n, h],
-                out.at[:, pl.ds(pl.multiple_of(h * HEAD_DIM, HEAD_DIM), HEAD_DIM)],
-                out_sem.at[n, h],
-            )
-            for n, (out, h) in enumerate(((dq_hbm, ahead), (dk_hbm, back), (dv_hbm, back)))
         ]
 
     def kv_copy(h, lag):
@@ -140,6 +153,71 @@
             device_id_type=MESH,
         )
 
+    class Exchange:
+        def __init__(self, slots, size, mine, device, send, recv):
+            self.slots, self.size, self.mine = slots, size, mine
+            self.device, self.send, self.recv = device, send, recv
+
+        def other(self, step):
+            return lax.rem(self.mine + step, self.size)
+
+        def copy(self, step, slot):
+            return pltpu.make_async_remote_copy(
+                src_ref=self.slots.at[slot],
+                dst_ref=self.slots.at[slot],
+                send_sem=self.send.at[step],
+                recv_sem=self.recv.at[slot],
+                device_id=self.device(self.other(step)),
+                device_id_type=MESH,
+            )
+
+        def greet(self):
+            @pl.loop(1, self.size)
+            def _(step):
+                pl.semaphore_signal(
+                    barrier, inc=1, device_id=self.device(self.other(step)), device_id_type=MESH
+                )
+
+        def start(self, value):
+            self.slots[self.mine] = value
+
+            @pl.loop(1, self.size)
+            def _(step):
+                self.copy(step, self.mine).start()
+
+        def receive(self):
+            @pl.loop(1, self.size)
+            def _(step):
+                self.copy(step, self.other(step)).wait_recv()
+
+        def total(self):
+            self.receive()
+            value = self.slots[0]
+            for slot in range(1, self.size):
+                value = value + self.slots[slot]
+            return value
+
+        def finish(self):
+            @pl.loop(1, self.size)
+            def _(step):
+                self.copy(step, self.mine).wait_send()
+
+    over_y = Exchange(tab_y, y_size, at_y, lambda y: at(at_z, y, at_core), y_send, y_recv)
+    over_z = Exchange(tab_z, z_size, at_z, lambda z: at(z, at_y, at_core), z_send, z_recv)
+    over_x = Exchange(tab_x, tp_size, tp, lambda x: (sp, x), x_send, x_recv)
+    other_core = at(at_z, at_y, 1 - at_core)
+    over_cores = Exchange(
+        tab_all, core_size, at_core, lambda core: at(at_z, at_y, core), all_send, all_recv
+    )
+    core_copy = pltpu.make_async_remote_copy(
+        src_ref=tab.at[pl.ds((1 - at_core) * GROUP, GROUP)],
+        dst_ref=tab_core,
+        send_sem=core_sem.at[0],
+        recv_sem=core_sem.at[1],
+        device_id=other_core,
+        device_id_type=MESH,
+    )
+
     stat_loads = [
         pltpu.make_async_copy(lse_hbm, stats.at[0, pl.ds(0, HEADS)], stat_sem.at[0]),
         pltpu.make_async_copy(dot_hbm, stats.at[0, pl.ds(HEADS, HEADS)], stat_sem.at[1]),
@@ -148,6 +226,8 @@
     barrier = pltpu.get_barrier_semaphore()
     for neighbour in (nxt, prv):
         pl.semaphore_signal(barrier, inc=1, device_id=neighbour, device_id_type=MESH)
+    for line in (over_z, over_y, over_x, over_cores):
+        line.greet()
 
     for copy in stat_loads:
         copy.start()
@@ -156,24 +236,6 @@
     def _(k):
         for copy in loads(k):
             copy.start()
-
-    pl.semaphore_wait(barrier, 2)
-
-    def await_loads(k):
-        for copy in loads(k):
-            copy.wait()
-
-    def send_own(k):
-        kv_copy(k, 0).start()
-        qg_copy(HEADS - 1 - k, 0).start()
-
-    for copy in stat_loads:
-        copy.wait()
-    st_copy(0).start()
-    for k in range(2):
-        await_loads(k)
-        send_own(k)
-    pl.loop(2, HEADS)(await_loads)
 
     ext[...] = jnp.broadcast_to(table_ref[:, TABLE_LEN - 1 : TABLE_LEN], (HEADS, 512))
     ext[:, 0:TABLE_LEN] = table_ref[...]
@@ -197,6 +259,24 @@
         flat = jnp.broadcast_to(row[:, 511:512], (HALF, HALF))
         bias[h, 3] = flat
         bias[h, 4] = jnp.where(far_off, -FAR, flat)
+
+    pl.semaphore_wait(barrier, z_size + y_size + tp_size + core_size - 2)
+
+    def await_loads(k):
+        for copy in loads(k):
+            copy.wait()
+
+    def send_own(k):
+        kv_copy(k, 0).start()
+        qg_copy(HEADS - 1 - k, 0).start()
+
+    for copy in stat_loads:
+        copy.wait()
+    st_copy(0).start()
+    for k in range(2):
+        await_loads(k)
+        send_own(k)
+    pl.loop(2, HEADS)(await_loads)
 
     st_copy(0).wait_recv()
     st_copy(1).start()
@@ -244,7 +324,7 @@
                 add_to(0, part, d, score_grads)
                 pieces.append(score_grads.astype(BF16))
             total_grads = dot_tn(jnp.concatenate(pieces, axis=0), keys)
-            outs[0, h, rows, :] = (total_grads * inv_root).astype(BF16)
+            dq_ref[rows, cols_of(h)] = (total_grads * inv_root).astype(BF16)
 
     def key_side(h):
         for part in range(2):
@@ -268,9 +348,9 @@
                 score_pieces.append(score_grads.astype(BF16))
                 weight_pieces.append(weights.astype(BF16))
             key_grads = dot_nn(jnp.concatenate(score_pieces, axis=1), queries)
-            outs[1, h, rows, :] = (key_grads * inv_root).astype(BF16)
+            dk_ref[rows, cols_of(h)] = (key_grads * inv_root).astype(BF16)
             value_grads = dot_nn(jnp.concatenate(weight_pieces, axis=1), grads)
-            outs[2, h, rows, :] = value_grads.astype(BF16)
+            dv_ref[rows, cols_of(h)] = value_grads.astype(BF16)
 
     def table_row(side, h):
         zeros = jnp.zeros((HALF, HALF), F32)
@@ -288,7 +368,8 @@
         clipped = (lane >= top) & (lane < 448)
         far = far + jnp.sum(jnp.where(clipped, by_distance, 0.0), keepdims=True)
         row = jnp.where(lane < top, by_distance, jnp.where(lane == top, far, 0.0))
-        gt_ref[pl.ds(h, 1), :] = row
+        for n in range(4):
+            tab[h, n : n + 1, :] = row[:, n * HALF : (n + 1) * HALF]
 
     @pl.loop(0, HEADS + 1)
     def _(k):
@@ -308,6 +389,24 @@
             ahead, back = k - 1, HEADS - k
             kv_copy(ahead, 1).wait_recv()
             query_side(ahead)
+
+            @pl.when(k == 5)
+            def _():
+                core_copy.wait_recv()
+                over_y.start(tab[pl.ds(at_core * GROUP, GROUP)] + tab_core[...])
+
+            @pl.when(k == 6)
+            def _():
+                over_z.start(over_y.total())
+
+            @pl.when(k == 7)
+            def _():
+                over_x.start(over_z.total())
+
+            @pl.when(k == 8)
+            def _():
+                over_cores.start(over_x.total())
+
             qg_copy(back, 1).wait_recv()
             key_side(back)
 
@@ -316,33 +415,45 @@
                 table_row(0, ahead)
                 table_row(1, back)
 
-            for copy in stores(ahead):
-                copy.start()
+            @pl.when(k == HEADS // 2)
+            def _():
+                core_copy.start()
+
+    over_cores.receive()
+    for h in range(HEADS):
+        for n in range(3):
+            width = min(HALF, TABLE_LEN - n * HALF)
+            gt_ref[h : h + 1, n * HALF : n * HALF + width] = tab_all[
+                h // GROUP, h % GROUP, n : n + 1, :width
+            ]
 
     @pl.loop(0, HEADS)
     def _(h):
         for lag in range(2):
             kv_copy(h, lag).wait_send()
             qg_copy(h, lag).wait_send()
-        for copy in stores(h):
-            copy.wait()
 
     st_copy(0).wait_send()
     st_copy(1).wait_send()
+    core_copy.wait_send()
+    for line in (over_y, over_z, over_x, over_cores):
+        line.finish()
 
 
 def solution(mesh):
     sp_size, tp_size = mesh.shape["sp"], mesh.shape["tp"]
 
     def local(query_rows, key_rows, value_rows, out_grad, log_totals, out_dot, bias_table):
-        hbm = pl.BlockSpec(memory_space=pl.ANY)
+        hbm = pl.BlockSpec(memory_space=pltpu.HBM)
+        z_size, y_size, core_size = SP_SHAPE
+        tiles = (GROUP, 4, HALF)
         vmem = pl.BlockSpec(memory_space=pltpu.VMEM)
         rows = jax.ShapeDtypeStruct(query_rows.shape, BF16)
-        grad_query, grad_key, grad_value, table_part = pl.pallas_call(
+        return pl.pallas_call(
             functools.partial(kernel, sp_size, tp_size),
-            out_shape=(rows, rows, rows, jax.ShapeDtypeStruct((HEADS, 512), F32)),
+            out_shape=(rows, rows, rows, jax.ShapeDtypeStruct(bias_table.shape, F32)),
             in_specs=[hbm] * 6 + [vmem],
-            out_specs=(hbm, hbm, hbm, vmem),
+            out_specs=(vmem, vmem, vmem, vmem),
             scratch_shapes=[
                 pltpu.VMEM((HEADS, 2, 3 * ROWS, HEAD_DIM), BF16),
                 pltpu.VMEM((HEADS, 2, 3 * ROWS, HEAD_DIM), BF16),
@@ -351,10 +462,23 @@
                 pltpu.VMEM((HEADS, 5, HALF, HALF), F32),
                 pltpu.VMEM((HEADS, 512), F32),
                 pltpu.VMEM((2, 5, HALF, HALF), F32),
-                pltpu.VMEM((3, HEADS, ROWS, HEAD_DIM), BF16),
+                pltpu.VMEM((HEADS, 4, HALF), F32),
+                pltpu.VMEM(tiles, F32),
+                pltpu.VMEM((y_size,) + tiles, F32),
+                pltpu.VMEM((z_size,) + tiles, F32),
+                pltpu.VMEM((tp_size,) + tiles, F32),
+                pltpu.VMEM((core_size,) + tiles, F32),
                 pltpu.SemaphoreType.DMA((4, HEADS)),
                 pltpu.SemaphoreType.DMA((2,)),
-                pltpu.SemaphoreType.DMA((3, HEADS)),
+                pltpu.SemaphoreType.DMA((2,)),
+                pltpu.SemaphoreType.DMA((y_size,)),
+                pltpu.SemaphoreType.DMA((y_size,)),
+                pltpu.SemaphoreType.DMA((z_size,)),
+                pltpu.SemaphoreType.DMA((z_size,)),
+                pltpu.SemaphoreType.DMA((tp_size,)),
+                pltpu.SemaphoreType.DMA((tp_size,)),
+                pltpu.SemaphoreType.DMA((core_size,)),
+                pltpu.SemaphoreType.DMA((core_size,)),
                 pltpu.SemaphoreType.DMA((2, HEADS)),
                 pltpu.SemaphoreType.DMA((2, HEADS)),
                 pltpu.SemaphoreType.DMA((2, HEADS)),
@@ -363,11 +487,9 @@
                 pltpu.SemaphoreType.DMA((2,)),
             ],
             compiler_params=pltpu.CompilerParams(
-                collective_id=0, has_side_effects=True
+                collective_id=0, has_side_effects=True, vmem_limit_bytes=32 * 2**20
             ),
         )(query_rows, key_rows, value_rows, out_grad, log_totals.T, out_dot.T, bias_table)
-        grad_table = lax.psum(table_part[:, :TABLE_LEN], ("sp", "tp"))
-        return grad_query, grad_key, grad_value, grad_table
 
     split = P(("sp", "tp"), None)
     return jax.shard_map(

time: 183 us -> 87.2 us (0.48)
  blocking collectives: 113 us -> 0 us
  Pallas kernels: 64.5 us -> 76.8 us
  local copies, waits for them, and re-layouts: 4.66 us -> 9.24 us
    psum x1 -> x0, blocking collectives: 113 us -> none  [local(): grad_table = lax.psum(table_part[:, :TABLE_LEN], ('sp', 'tp'))]
    pallas_call x1, Pallas kernels: 64.5 us -> 76.8 us  [local(): pl.pallas_call(functools.partial(kernel, sp_size, tp_size), out_shape=(ro...]
    unnamed x7 -> x18, local copies, waits for them, and re-layouts: 3.95 us -> 9.24 us
where the time goes in v2:
time: 87.2 us; the launch traced here: 86.7 us
  Pallas kernels  76.8 us (88%)
  local copies, waits for them, and re-layouts  9.24 us (11%)
    pallas_call x1, Pallas kernels, local(): pl.pallas_call(functools.partial(kernel, sp_size, tp_size), out_shape=(ro...  76.8 us
    unnamed x18, local copies, waits for them, and re-layouts  9.24 us

profile of v2, /device:TPU:1, one launch (start us, length us, event | category | flops | bytes accessed | tf_op | source)
XLA Modules:
  0.0 86.7 jit_solution(16159117771773776115)
XLA Ops:
  0.6 0.0 copy-start
  0.6 1.0 %copy-done = bf16[256,1024]{1,0:T(8,128)(2,1)S(1)} copy-done((bf16[256,1024]{1,0:T(8,128)(2,1)S(1)}, bf16[256,1024]{1,0:T(8,128)(2,1)}, u32[]{:S(2)}) %copy-start) | copy-done | bytes 524312
  1.7 0.0 copy-start.1
  1.7 1.0 %copy-done.1 = bf16[256,1024]{1,0:T(8,128)(2,1)S(1)} copy-done((bf16[256,1024]{1,0:T(8,128)(2,1)S(1)}, bf16[256,1024]{1,0:T(8,128)(2,1)}, u32[]{:S(2)}) %copy-start.1) | copy-done | bytes 524312
  2.7 0.0 copy-start.2
  2.7 1.0 %copy-done.2 = bf16[256,1024]{1,0:T(8,128)(2,1)S(1)} copy-done((bf16[256,1024]{1,0:T(8,128)(2,1)S(1)}, bf16[256,1024]{1,0:T(8,128)(2,1)}, u32[]{:S(2)}) %copy-start.2) | copy-done | bytes 524312
  3.8 0.0 copy-start.3
  3.8 1.0 %copy-done.3 = bf16[256,1024]{1,0:T(8,128)(2,1)S(1)} copy-done((bf16[256,1024]{1,0:T(8,128)(2,1)S(1)}, bf16[256,1024]{1,0:T(8,128)(2,1)}, u32[]{:S(2)}) %copy-start.3) | copy-done | bytes 524312
  4.8 0.0 copy-start.4
  4.8 0.7 copy-done.4
  5.5 0.0 copy-start.5
  5.5 0.7 copy-done.5
  6.2 0.0 copy-start.6
  6.2 0.7 copy-done.6
  6.9 76.8 %shard_map.102 = (bf16[256,1024]{1,0:T(8,128)(2,1)S(1)}, bf16[256,1024]{1,0:T(8,128)(2,1)S(1)}, bf16[256,1024]{1,0:T(8,128)(2,1)S(1)}, f32[8,320]{1,0:T(8,128)S(1)}) custom-call(bf16[256,1024]{1,0:T(8,128)(2,1)S(1)} %copy-done, bf16[256,1024]{1,0:T(8,128)(2,1)S(1)} %copy-done.1, bf16[256,1024]{1,0:T(8,128)(2,1)S(1)} %copy-done.2, ...), custom_call_target="tpu_custom_call" | custom-call | tf_op jit(solution)/shard_map/pallas_call | solution.py:452
  83.7 0.8 copy.15
  84.5 0.8 copy.16
  85.3 0.8 copy.17
  86.1 0.6 copy.18
Async XLA Ops:
  0.6 1.0 %copy-start = (bf16[256,1024]{1,0:T(8,128)(2,1)S(1)}, bf16[256,1024]{1,0:T(8,128)(2,1)}, u32[]{:S(2)}) copy-start(bf16[256,1024]{1,0:T(8,128)(2,1)} %q_hbm.1) | copy-start | bytes 1572868
  1.7 1.0 %copy-start.1 = (bf16[256,1024]{1,0:T(8,128)(2,1)S(1)}, bf16[256,1024]{1,0:T(8,128)(2,1)}, u32[]{:S(2)}) copy-start(bf16[256,1024]{1,0:T(8,128)(2,1)} %k_hbm.1) | copy-start | bytes 1572868
  2.7 1.0 %copy-start.2 = (bf16[256,1024]{1,0:T(8,128)(2,1)S(1)}, bf16[256,1024]{1,0:T(8,128)(2,1)}, u32[]{:S(2)}) copy-start(bf16[256,1024]{1,0:T(8,128)(2,1)} %v_hbm.1) | copy-start | bytes 1572868
  3.8 1.0 %copy-start.3 = (bf16[256,1024]{1,0:T(8,128)(2,1)S(1)}, bf16[256,1024]{1,0:T(8,128)(2,1)}, u32[]{:S(2)}) copy-start(bf16[256,1024]{1,0:T(8,128)(2,1)} %g_hbm.1) | copy-start | bytes 1572868
  4.8 0.7 copy-start.4
  5.5 0.7 copy-start.5
  6.2 0.7 copy-start.6

commit v3 on v2

--- a/solution.py
+++ b/solution.py
@@ -46,7 +46,7 @@
     g_hbm,
     lse_hbm,
     dot_hbm,
-    table_ref,
+    table_hbm,
     dq_ref,
     dk_ref,
     dv_ref,
@@ -56,6 +56,7 @@
     stats,
     wide,
     bias,
+    table_ref,
     ext,
     acc,
     tab,
@@ -66,6 +67,7 @@
     tab_all,
     load_sem,
     stat_sem,
+    chain,
     core_sem,
     y_send,
     y_recv,
@@ -171,13 +173,6 @@
                 device_id_type=MESH,
             )
 
-        def greet(self):
-            @pl.loop(1, self.size)
-            def _(step):
-                pl.semaphore_signal(
-                    barrier, inc=1, device_id=self.device(self.other(step)), device_id_type=MESH
-                )
-
         def start(self, value):
             self.slots[self.mine] = value
 
@@ -222,13 +217,61 @@
         pltpu.make_async_copy(lse_hbm, stats.at[0, pl.ds(0, HEADS)], stat_sem.at[0]),
         pltpu.make_async_copy(dot_hbm, stats.at[0, pl.ds(HEADS, HEADS)], stat_sem.at[1]),
     ]
+    table_load = pltpu.make_async_copy(table_hbm, table_ref, stat_sem.at[2])
+
+    has_prv, has_nxt = me >= 1, me + 1 < total
+    has_prv2, has_nxt2 = me >= 2, me + 2 < total
+    y_low, y_high = lax.rem(at_y + y_size - 1, y_size), lax.rem(at_y + 1, y_size)
+    z_low, z_high = lax.rem(at_z + z_size - 1, z_size), lax.rem(at_z + 1, z_size)
+    lines = (
+        (at(at_z, y_low, at_core), at(at_z, y_high, at_core), y_size > 2, y_size > 1),
+        (at(z_low, at_y, at_core), at(z_high, at_y, at_core), at_z > 0, at_z < z_size - 1),
+    )
+    near = [(nxt, has_nxt), (prv, has_prv), (other_core, True)]
+    near += [((sp, lax.rem(tp + step, tp_size)), True) for step in range(1, tp_size)]
+    for low, high, has_low, has_high in lines:
+        near += [(low, has_low), (high, has_high)]
+    greeted = sum(jnp.where(cond, 1, 0) for _, cond in near)
+
+    def tell(line):
+        low, high, has_low, has_high = lines[line]
+
+        @pl.when(has_low)
+        def _():
+            pl.semaphore_signal(
+                chain.at[2 * line + 1], inc=1, device_id=low, device_id_type=MESH
+            )
+
+        @pl.when(has_high)
+        def _():
+            pl.semaphore_signal(chain.at[2 * line], inc=1, device_id=high, device_id_type=MESH)
+
+    def hear(line):
+        _, _, has_low, has_high = lines[line]
+
+        @pl.when(has_low)
+        def _():
+            pl.semaphore_wait(chain.at[2 * line], 1)
+
+        @pl.when(has_high)
+        def _():
+            pl.semaphore_wait(chain.at[2 * line + 1], 1)
+
+    y_rounds, z_rounds = max(y_size // 2 - 1, 0), max(z_size - 2, 0)
+
+    def in_round(line, cond, act):
+        @pl.when(cond)
+        def _():
+            act(line)
 
     barrier = pltpu.get_barrier_semaphore()
-    for neighbour in (nxt, prv):
-        pl.semaphore_signal(barrier, inc=1, device_id=neighbour, device_id_type=MESH)
-    for line in (over_z, over_y, over_x, over_cores):
-        line.greet()
-
+    for device, cond in near:
+
+        @pl.when(cond)
+        def _():
+            pl.semaphore_signal(barrier, inc=1, device_id=device, device_id_type=MESH)
+
+    table_load.start()
     for copy in stat_loads:
         copy.start()
 
@@ -237,6 +280,7 @@
         for copy in loads(k):
             copy.start()
 
+    table_load.wait()
     ext[...] = jnp.broadcast_to(table_ref[:, TABLE_LEN - 1 : TABLE_LEN], (HEADS, 512))
     ext[:, 0:TABLE_LEN] = table_ref[...]
     ext[...] = pltpu.roll(ext[...], 65, 1) * LOG2E
@@ -260,27 +304,73 @@
         bias[h, 3] = flat
         bias[h, 4] = jnp.where(far_off, -FAR, flat)
 
-    pl.semaphore_wait(barrier, z_size + y_size + tp_size + core_size - 2)
+    pl.semaphore_wait(barrier, greeted)
 
     def await_loads(k):
         for copy in loads(k):
             copy.wait()
 
-    def send_own(k):
-        kv_copy(k, 0).start()
-        qg_copy(HEADS - 1 - k, 0).start()
+    def send_kv(k):
+        @pl.when(has_nxt)
+        def _():
+            kv_copy(k, 0).start()
+
+    def send_qg(k):
+        @pl.when(has_prv)
+        def _():
+            qg_copy(HEADS - 1 - k, 0).start()
 
     for copy in stat_loads:
         copy.wait()
-    st_copy(0).start()
+
+    @pl.when(has_prv)
+    def _():
+        st_copy(0).start()
+
     for k in range(2):
         await_loads(k)
-        send_own(k)
+        send_kv(k)
+        send_qg(k)
     pl.loop(2, HEADS)(await_loads)
 
-    st_copy(0).wait_recv()
-    st_copy(1).start()
-    st_copy(1).wait_recv()
+    def clear(buffer, start, rows):
+        @pl.loop(0, HEADS)
+        def _(h):
+            for n in range(2):
+                buffer[h, n, start : start + rows, :] = jnp.zeros((rows, HEAD_DIM), BF16)
+
+    @pl.when(jnp.logical_not(has_prv))
+    def _():
+        pl.loop(2, HEADS)(send_kv)
+        clear(kv, 0, 2 * ROWS)
+
+    @pl.when(jnp.logical_not(has_nxt))
+    def _():
+        pl.loop(2, HEADS)(send_qg)
+        clear(qg, ROWS, 2 * ROWS)
+        stats[1] = jnp.zeros((2 * HEADS, ROWS), F32)
+        stats[2] = jnp.zeros((2 * HEADS, ROWS), F32)
+
+    @pl.when(me == 1)
+    def _():
+        clear(kv, 0, ROWS)
+
+    @pl.when(me + 2 == total)
+    def _():
+        clear(qg, 2 * ROWS, ROWS)
+        stats[2] = jnp.zeros((2 * HEADS, ROWS), F32)
+
+    @pl.when(has_nxt)
+    def _():
+        st_copy(0).wait_recv()
+
+        @pl.when(has_prv)
+        def _():
+            st_copy(1).start()
+
+    @pl.when(has_nxt2)
+    def _():
+        st_copy(1).wait_recv()
 
     def off(cond):
         return jnp.where(cond, FAR, 0.0).astype(F32)
@@ -373,41 +463,62 @@
 
     @pl.loop(0, HEADS + 1)
     def _(k):
-        @pl.when(k < HEADS)
+        in_round(0, k < y_rounds, tell)
+        in_round(1, 2 * k < z_rounds, tell)
+
+        @pl.when((k < HEADS) & has_prv)
         def _():
             kv_copy(k, 0).wait_recv()
-            kv_copy(k, 1).start()
+
+            @pl.when(has_nxt)
+            def _():
+                kv_copy(k, 1).start()
+
+        @pl.when((k < HEADS) & has_nxt)
+        def _():
             qg_copy(HEADS - 1 - k, 0).wait_recv()
-            qg_copy(HEADS - 1 - k, 1).start()
-
-        @pl.when(k < HEADS - 2)
-        def _():
-            send_own(k + 2)
+
+            @pl.when(has_prv)
+            def _():
+                qg_copy(HEADS - 1 - k, 1).start()
+
+        @pl.when((k < HEADS - 2) & has_prv)
+        def _():
+            send_kv(k + 2)
+
+        @pl.when((k < HEADS - 2) & has_nxt)
+        def _():
+            send_qg(k + 2)
+
+        in_round(1, 2 * k < z_rounds, hear)
+        in_round(1, 2 * k + 1 < z_rounds, tell)
 
         @pl.when(k >= 1)
         def _():
             ahead, back = k - 1, HEADS - k
-            kv_copy(ahead, 1).wait_recv()
+
+            @pl.when(has_prv2)
+            def _():
+                kv_copy(ahead, 1).wait_recv()
+
             query_side(ahead)
 
             @pl.when(k == 5)
             def _():
-                core_copy.wait_recv()
-                over_y.start(tab[pl.ds(at_core * GROUP, GROUP)] + tab_core[...])
+                over_z.start(over_y.total())
 
             @pl.when(k == 6)
             def _():
-                over_z.start(over_y.total())
+                over_x.start(over_z.total())
 
             @pl.when(k == 7)
             def _():
-                over_x.start(over_z.total())
-
-            @pl.when(k == 8)
-            def _():
                 over_cores.start(over_x.total())
 
-            qg_copy(back, 1).wait_recv()
+            @pl.when(has_nxt2)
+            def _():
+                qg_copy(back, 1).wait_recv()
+
             key_side(back)
 
             @pl.when(k <= HEADS // 2)
@@ -415,9 +526,14 @@
                 table_row(0, ahead)
                 table_row(1, back)
 
-            @pl.when(k == HEADS // 2)
-            def _():
-                core_copy.start()
+        in_round(0, k < y_rounds, hear)
+        in_round(1, 2 * k + 1 < z_rounds, hear)
+
+        @pl.when(k == HEADS // 2)
+        def _():
+            core_copy.start()
+            core_copy.wait_recv()
+            over_y.start(tab[pl.ds(at_core * GROUP, GROUP)] + tab_core[...])
 
     over_cores.receive()
     for h in range(HEADS):
@@ -427,17 +543,46 @@
                 h // GROUP, h % GROUP, n : n + 1, :width
             ]
 
-    @pl.loop(0, HEADS)
-    def _(h):
-        for lag in range(2):
-            kv_copy(h, lag).wait_send()
-            qg_copy(h, lag).wait_send()
-
-    st_copy(0).wait_send()
-    st_copy(1).wait_send()
+    @pl.when(has_nxt)
+    def _():
+        @pl.loop(0, HEADS)
+        def _(h):
+            kv_copy(h, 0).wait_send()
+
+            @pl.when(has_prv)
+            def _():
+                kv_copy(h, 1).wait_send()
+
+    @pl.when(has_prv)
+    def _():
+        st_copy(0).wait_send()
+
+        @pl.when(has_nxt)
+        def _():
+            st_copy(1).wait_send()
+
+        @pl.loop(0, HEADS)
+        def _(h):
+            qg_copy(h, 0).wait_send()
+
+            @pl.when(has_nxt)
+            def _():
+                qg_copy(h, 1).wait_send()
+
     core_copy.wait_send()
     for line in (over_y, over_z, over_x, over_cores):
         line.finish()
+
+
+def write_out(*refs):
+    count = len(refs) // 2
+    copies = [
+        pltpu.make_async_copy(refs[n], refs[count + n], refs[-1].at[n]) for n in range(count)
+    ]
+    for copy in copies:
+        copy.start()
+    for copy in copies:
+        copy.wait()
 
 
 def solution(mesh):
@@ -447,12 +592,17 @@
         hbm = pl.BlockSpec(memory_space=pltpu.HBM)
         z_size, y_size, core_size = SP_SHAPE
         tiles = (GROUP, 4, HALF)
+
+        def in_hbm(array):
+            return pltpu.with_memory_space_constraint(array, pltpu.HBM)
+
         vmem = pl.BlockSpec(memory_space=pltpu.VMEM)
         rows = jax.ShapeDtypeStruct(query_rows.shape, BF16)
-        return pl.pallas_call(
+        shapes = (rows, rows, rows, jax.ShapeDtypeStruct(bias_table.shape, F32))
+        results = pl.pallas_call(
             functools.partial(kernel, sp_size, tp_size),
-            out_shape=(rows, rows, rows, jax.ShapeDtypeStruct(bias_table.shape, F32)),
-            in_specs=[hbm] * 6 + [vmem],
+            out_shape=shapes,
+            in_specs=[hbm] * 7,
             out_specs=(vmem, vmem, vmem, vmem),
             scratch_shapes=[
                 pltpu.VMEM((HEADS, 2, 3 * ROWS, HEAD_DIM), BF16),
@@ -460,6 +610,7 @@
                 pltpu.VMEM((3, 2 * HEADS, ROWS), F32),
                 pltpu.VMEM((3, 2 * HEADS, 8, ROWS), F32),
                 pltpu.VMEM((HEADS, 5, HALF, HALF), F32),
+                pltpu.VMEM((HEADS, TABLE_LEN), F32),
                 pltpu.VMEM((HEADS, 512), F32),
                 pltpu.VMEM((2, 5, HALF, HALF), F32),
                 pltpu.VMEM((HEADS, 4, HALF), F32),
@@ -469,7 +620,8 @@
                 pltpu.VMEM((tp_size,) + tiles, F32),
                 pltpu.VMEM((core_size,) + tiles, F32),
                 pltpu.SemaphoreType.DMA((4, HEADS)),
-                pltpu.SemaphoreType.DMA((2,)),
+                pltpu.SemaphoreType.DMA((3,)),
+                pltpu.SemaphoreType.REGULAR((4,)),
                 pltpu.SemaphoreType.DMA((2,)),
                 pltpu.SemaphoreType.DMA((y_size,)),
                 pltpu.SemaphoreType.DMA((y_size,)),
@@ -489,7 +641,14 @@
             compiler_params=pltpu.CompilerParams(
                 collective_id=0, has_side_effects=True, vmem_limit_bytes=32 * 2**20
             ),
-        )(query_rows, key_rows, value_rows, out_grad, log_totals.T, out_dot.T, bias_table)
+        )(*map(in_hbm, (query_rows, key_rows, value_rows, out_grad, log_totals.T, out_dot.T, bias_table)))
+        return pl.pallas_call(
+            write_out,
+            out_shape=shapes,
+            in_specs=[vmem] * 4,
+            out_specs=(hbm,) * 4,
+            scratch_shapes=[pltpu.SemaphoreType.DMA((4,))],
+        )(*(pltpu.with_memory_space_constraint(part, pltpu.VMEM) for part in results))
 
     split = P(("sp", "tp"), None)
     return jax.shard_map(

time: 87.2 us -> 75.9 us (0.87)
  local copies, waits for them, and re-layouts: 9.24 us -> 0 us
  Pallas kernels: 76.8 us -> 75.1 us
    unnamed x18 -> x0, local copies, waits for them, and re-layouts: 9.24 us -> none
    pallas_call x1 -> x2, Pallas kernels: 76.8 us -> 75.1 us  [the longest x1 73.9 us: local(): pl.pallas_call(functools.partial(kernel, sp_size, tp_size), out_shape=sha...]
where the time goes in v3:
time: 75.9 us; the launch traced here: 75.8 us
  Pallas kernels  75.1 us (99%)
    pallas_call x1, Pallas kernels, local(): pl.pallas_call(functools.partial(kernel, sp_size, tp_size), out_shape=sha...  73.9 us

profile of v3, /device:TPU:1, one launch (start us, length us, event | category | flops | bytes accessed | tf_op | source)
XLA Modules:
  0.0 75.8 jit_solution(9045604157353846410)
XLA Ops:
  0.6 73.9 %shard_map.102 = (bf16[256,1024]{1,0:T(8,128)(2,1)S(1)}, bf16[256,1024]{1,0:T(8,128)(2,1)S(1)}, bf16[256,1024]{1,0:T(8,128)(2,1)S(1)}, f32[8,320]{1,0:T(8,128)S(1)}) custom-call(bf16[256,1024]{1,0:T(8,128)(2,1)} %q_hbm.1, bf16[256,1024]{1,0:T(8,128)(2,1)} %k_hbm.1, bf16[256,1024]{1,0:T(8,128)(2,1)} %v_hbm.1, bf16[256,1024]{1,0:T(8,128)(2,1)} %g_hbm.1, ...), custom_call_target="tpu_custom_call" | custom-call | tf_op jit(solution)/shard_map/pallas_call | solution.py:602
  74.6 1.2 %shard_map.103 = (bf16[256,1024]{1,0:T(8,128)(2,1)}, bf16[256,1024]{1,0:T(8,128)(2,1)}, bf16[256,1024]{1,0:T(8,128)(2,1)}, f32[8,320]{1,0:T(8,128)}) custom-call(bf16[256,1024]{1,0:T(8,128)(2,1)S(1)} %get-tuple-element.8.refs_0_, bf16[256,1024]{1,0:T(8,128)(2,1)S(1)} %get-tuple-element.9.refs_1_, bf16[256,1024]{1,0:T(8,128)(2,1)S(1)} %get-tuple-element.10.refs_2_, ...), custom_call_target="tpu_custom_call" | custom-call | tf_op jit(solution)/shard_map/pallas_call | solution.py:645

commit v4 on v3

--- a/solution.py
+++ b/solution.py
@@ -461,34 +461,48 @@
         for n in range(4):
             tab[h, n : n + 1, :] = row[:, n * HALF : (n + 1) * HALF]
 
+    def forward(k):
+        @pl.when(has_prv)
+        def _():
+            kv_copy(k, 0).wait_recv()
+
+            @pl.when(has_nxt)
+            def _():
+                kv_copy(k, 1).start()
+
+        @pl.when(has_nxt)
+        def _():
+            qg_copy(HEADS - 1 - k, 0).wait_recv()
+
+            @pl.when(has_prv)
+            def _():
+                qg_copy(HEADS - 1 - k, 1).start()
+
+    def send_own(k):
+        @pl.when(has_prv)
+        def _():
+            send_kv(k)
+
+        @pl.when(has_nxt)
+        def _():
+            send_qg(k)
+
     @pl.loop(0, HEADS + 1)
     def _(k):
         in_round(0, k < y_rounds, tell)
         in_round(1, 2 * k < z_rounds, tell)
 
-        @pl.when((k < HEADS) & has_prv)
-        def _():
-            kv_copy(k, 0).wait_recv()
-
-            @pl.when(has_nxt)
-            def _():
-                kv_copy(k, 1).start()
-
-        @pl.when((k < HEADS) & has_nxt)
-        def _():
-            qg_copy(HEADS - 1 - k, 0).wait_recv()
-
-            @pl.when(has_prv)
-            def _():
-                qg_copy(HEADS - 1 - k, 1).start()
-
-        @pl.when((k < HEADS - 2) & has_prv)
-        def _():
-            send_kv(k + 2)
-
-        @pl.when((k < HEADS - 2) & has_nxt)
-        def _():
-            send_qg(k + 2)
+        @pl.when(k < GROUP)
+        def _():
+            forward(k)
+
+        @pl.when(k < 2)
+        def _():
+            send_own(k + 2)
+
+        @pl.when(k == 3)
+        def _():
+            send_own(4)
 
         in_round(1, 2 * k < z_rounds, hear)
         in_round(1, 2 * k + 1 < z_rounds, tell)
@@ -503,17 +517,9 @@
 
             query_side(ahead)
 
-            @pl.when(k == 5)
-            def _():
-                over_z.start(over_y.total())
-
-            @pl.when(k == 6)
-            def _():
-                over_x.start(over_z.total())
-
-            @pl.when(k == 7)
-            def _():
-                over_cores.start(over_x.total())
+            @pl.when(k == HEADS)
+            def _():
+                over_cores.start(over_z.total())
 
             @pl.when(has_nxt2)
             def _():
@@ -521,7 +527,7 @@
 
             key_side(back)
 
-            @pl.when(k <= HEADS // 2)
+            @pl.when(k <= GROUP)
             def _():
                 table_row(0, ahead)
                 table_row(1, back)
@@ -529,11 +535,17 @@
         in_round(0, k < y_rounds, hear)
         in_round(1, 2 * k + 1 < z_rounds, hear)
 
-        @pl.when(k == HEADS // 2)
-        def _():
+        @pl.when(k == GROUP)
+        def _():
+            over_x.start(tab[...])
+            pl.loop(5, HEADS)(send_own)
+            forward(4)
+            tab[...] = over_x.total()
             core_copy.start()
             core_copy.wait_recv()
             over_y.start(tab[pl.ds(at_core * GROUP, GROUP)] + tab_core[...])
+            pl.loop(5, HEADS)(forward)
+            over_z.start(over_y.total())
 
     over_cores.receive()
     for h in range(HEADS):
@@ -617,7 +629,7 @@
                 pltpu.VMEM(tiles, F32),
                 pltpu.VMEM((y_size,) + tiles, F32),
                 pltpu.VMEM((z_size,) + tiles, F32),
-                pltpu.VMEM((tp_size,) + tiles, F32),
+                pltpu.VMEM((tp_size, HEADS) + tiles[1:], F32),
                 pltpu.VMEM((core_size,) + tiles, F32),
                 pltpu.SemaphoreType.DMA((4, HEADS)),
                 pltpu.SemaphoreType.DMA((3,)),

time: 75.9 us -> 73.5 us (0.968)
  Pallas kernels: 75.1 us -> 72.7 us
    pallas_call x1, Pallas kernels: 73.9 us -> 71.5 us  [local(): pl.pallas_call(functools.partial(kernel, sp_size, tp_size), out_shape=sha...]
where the time goes in v4:
time: 73.5 us; the launch traced here: 73.4 us
  Pallas kernels  72.7 us (99%)
    pallas_call x1, Pallas kernels, local(): pl.pallas_call(functools.partial(kernel, sp_size, tp_size), out_shape=sha...  71.5 us

profile of v4, /device:TPU:1, one launch (start us, length us, event | category | flops | bytes accessed | tf_op | source)
XLA Modules:
  0.0 73.4 jit_solution(14803758311247958507)
XLA Ops:
  0.6 71.5 %shard_map.102 = (bf16[256,1024]{1,0:T(8,128)(2,1)S(1)}, bf16[256,1024]{1,0:T(8,128)(2,1)S(1)}, bf16[256,1024]{1,0:T(8,128)(2,1)S(1)}, f32[8,320]{1,0:T(8,128)S(1)}) custom-call(bf16[256,1024]{1,0:T(8,128)(2,1)} %q_hbm.1, bf16[256,1024]{1,0:T(8,128)(2,1)} %k_hbm.1, bf16[256,1024]{1,0:T(8,128)(2,1)} %v_hbm.1, bf16[256,1024]{1,0:T(8,128)(2,1)} %g_hbm.1, ...), custom_call_target="tpu_custom_call" | custom-call | tf_op jit(solution)/shard_map/pallas_call | solution.py:614
  72.2 1.2 %shard_map.103 = (bf16[256,1024]{1,0:T(8,128)(2,1)}, bf16[256,1024]{1,0:T(8,128)(2,1)}, bf16[256,1024]{1,0:T(8,128)(2,1)}, f32[8,320]{1,0:T(8,128)}) custom-call(bf16[256,1024]{1,0:T(8,128)(2,1)S(1)} %get-tuple-element.8.refs_0_, bf16[256,1024]{1,0:T(8,128)(2,1)S(1)} %get-tuple-element.9.refs_1_, bf16[256,1024]{1,0:T(8,128)(2,1)S(1)} %get-tuple-element.10.refs_2_, ...), custom_call_target="tpu_custom_call" | custom-call | tf_op jit(solution)/shard_map/pallas_call | solution.py:657

commit v5 on v4

--- a/solution.py
+++ b/solution.py
@@ -60,11 +60,11 @@
     ext,
     acc,
     tab,
+    tab_half,
     tab_core,
     tab_y,
     tab_z,
-    tab_x,
-    tab_all,
+    tab_row,
     load_sem,
     stat_sem,
     chain,
@@ -73,10 +73,8 @@
     y_recv,
     z_send,
     z_recv,
-    x_send,
-    x_recv,
-    all_send,
-    all_recv,
+    row_send,
+    row_recv,
     kv_send,
     kv_recv,
     qg_send,
@@ -199,13 +197,18 @@
 
     over_y = Exchange(tab_y, y_size, at_y, lambda y: at(at_z, y, at_core), y_send, y_recv)
     over_z = Exchange(tab_z, z_size, at_z, lambda z: at(z, at_y, at_core), z_send, z_recv)
-    over_x = Exchange(tab_x, tp_size, tp, lambda x: (sp, x), x_send, x_recv)
+    row_size = core_size * tp_size
+    over_row = Exchange(
+        tab_row,
+        row_size,
+        at_core * tp_size + tp,
+        lambda e: (at(at_z, at_y, e // tp_size)[0], lax.rem(e, tp_size)),
+        row_send,
+        row_recv,
+    )
     other_core = at(at_z, at_y, 1 - at_core)
-    over_cores = Exchange(
-        tab_all, core_size, at_core, lambda core: at(at_z, at_y, core), all_send, all_recv
-    )
     core_copy = pltpu.make_async_remote_copy(
-        src_ref=tab.at[pl.ds((1 - at_core) * GROUP, GROUP)],
+        src_ref=tab_half.at[1 - at_core],
         dst_ref=tab_core,
         send_sem=core_sem.at[0],
         recv_sem=core_sem.at[1],
@@ -227,8 +230,8 @@
         (at(at_z, y_low, at_core), at(at_z, y_high, at_core), y_size > 2, y_size > 1),
         (at(z_low, at_y, at_core), at(z_high, at_y, at_core), at_z > 0, at_z < z_size - 1),
     )
-    near = [(nxt, has_nxt), (prv, has_prv), (other_core, True)]
-    near += [((sp, lax.rem(tp + step, tp_size)), True) for step in range(1, tp_size)]
+    near = [(nxt, has_nxt), (prv, has_prv)]
+    near += [(over_row.device(over_row.other(step)), True) for step in range(1, row_size)]
     for low, high, has_low, has_high in lines:
         near += [(low, has_low), (high, has_high)]
     greeted = sum(jnp.where(cond, 1, 0) for _, cond in near)
@@ -500,9 +503,9 @@
         def _():
             send_own(k + 2)
 
-        @pl.when(k == 3)
-        def _():
-            send_own(4)
+        @pl.when(k == GROUP - 1)
+        def _():
+            pl.loop(GROUP, HEADS)(send_own)
 
         in_round(1, 2 * k < z_rounds, hear)
         in_round(1, 2 * k + 1 < z_rounds, tell)
@@ -517,9 +520,9 @@
 
             query_side(ahead)
 
-            @pl.when(k == HEADS)
-            def _():
-                over_cores.start(over_z.total())
+            @pl.when(k == HEADS - 1)
+            def _():
+                over_row.start(over_z.total())
 
             @pl.when(has_nxt2)
             def _():
@@ -537,23 +540,27 @@
 
         @pl.when(k == GROUP)
         def _():
-            over_x.start(tab[...])
-            pl.loop(5, HEADS)(send_own)
-            forward(4)
-            tab[...] = over_x.total()
+            for h in range(HEADS):
+                half, row = h // GROUP, 3 * (h % GROUP)
+                tab_half[half, row : row + 3, :] = tab[h, 0:3, :]
             core_copy.start()
             core_copy.wait_recv()
-            over_y.start(tab[pl.ds(at_core * GROUP, GROUP)] + tab_core[...])
-            pl.loop(5, HEADS)(forward)
+            over_y.start(tab_half[at_core] + tab_core[...])
+            pl.loop(GROUP, 6)(forward)
             over_z.start(over_y.total())
-
-    over_cores.receive()
-    for h in range(HEADS):
-        for n in range(3):
-            width = min(HALF, TABLE_LEN - n * HALF)
-            gt_ref[h : h + 1, n * HALF : n * HALF + width] = tab_all[
-                h // GROUP, h % GROUP, n : n + 1, :width
-            ]
+            pl.loop(6, HEADS)(forward)
+
+    over_row.receive()
+    for half in range(2):
+        value = tab_row[half * tp_size]
+        for x in range(1, tp_size):
+            value = value + tab_row[half * tp_size + x]
+        for h in range(GROUP):
+            for n in range(3):
+                width = min(HALF, TABLE_LEN - n * HALF)
+                gt_ref[
+                    half * GROUP + h : half * GROUP + h + 1, n * HALF : n * HALF + width
+                ] = value[3 * h + n : 3 * h + n + 1, :width]
 
     @pl.when(has_nxt)
     def _():
@@ -582,7 +589,7 @@
                 qg_copy(h, 1).wait_send()
 
     core_copy.wait_send()
-    for line in (over_y, over_z, over_x, over_cores):
+    for line in (over_y, over_z, over_row):
         line.finish()
 
 
@@ -603,7 +610,7 @@
     def local(query_rows, key_rows, value_rows, out_grad, log_totals, out_dot, bias_table):
         hbm = pl.BlockSpec(memory_space=pltpu.HBM)
         z_size, y_size, core_size = SP_SHAPE
-        tiles = (GROUP, 4, HALF)
+        tiles = (3 * GROUP, HALF)
 
         def in_hbm(array):
             return pltpu.with_memory_space_constraint(array, pltpu.HBM)
@@ -626,11 +633,11 @@
                 pltpu.VMEM((HEADS, 512), F32),
                 pltpu.VMEM((2, 5, HALF, HALF), F32),
                 pltpu.VMEM((HEADS, 4, HALF), F32),
+                pltpu.VMEM((2,) + tiles, F32),
                 pltpu.VMEM(tiles, F32),
                 pltpu.VMEM((y_size,) + tiles, F32),
                 pltpu.VMEM((z_size,) + tiles, F32),
-                pltpu.VMEM((tp_size, HEADS) + tiles[1:], F32),
-                pltpu.VMEM((core_size,) + tiles, F32),
+                pltpu.VMEM((core_size * tp_size,) + tiles, F32),
                 pltpu.SemaphoreType.DMA((4, HEADS)),
                 pltpu.SemaphoreType.DMA((3,)),
                 pltpu.SemaphoreType.REGULAR((4,)),
@@ -639,10 +646,8 @@
                 pltpu.SemaphoreType.DMA((y_size,)),
                 pltpu.SemaphoreType.DMA((z_size,)),
                 pltpu.SemaphoreType.DMA((z_size,)),
-                pltpu.SemaphoreType.DMA((tp_size,)),
-                pltpu.SemaphoreType.DMA((tp_size,)),
-                pltpu.SemaphoreType.DMA((core_size,)),
-                pltpu.SemaphoreType.DMA((core_size,)),
+                pltpu.SemaphoreType.DMA((core_size * tp_size,)),
+                pltpu.SemaphoreType.DMA((core_size * tp_size,)),
                 pltpu.SemaphoreType.DMA((2, HEADS)),
                 pltpu.SemaphoreType.DMA((2, HEADS)),
                 pltpu.SemaphoreType.DMA((2, HEADS)),

time: 73.5 us -> 71.8 us (0.977)
  Pallas kernels: 72.7 us -> 70.8 us
    pallas_call x1, Pallas kernels: 71.5 us -> 69.6 us  [local(): pl.pallas_call(functools.partial(kernel, sp_size, tp_size), out_shape=sha...]
where the time goes in v5:
time: 71.8 us; the launch traced here: 71.4 us
  Pallas kernels  70.8 us (99%)
    pallas_call x1, Pallas kernels, local(): pl.pallas_call(functools.partial(kernel, sp_size, tp_size), out_shape=sha...  69.6 us

profile of v5, /device:TPU:1, one launch (start us, length us, event | category | flops | bytes accessed | tf_op | source)
XLA Modules:
  0.0 71.4 jit_solution(10613957826905525349)
XLA Ops:
  0.6 69.6 %shard_map.102 = (bf16[256,1024]{1,0:T(8,128)(2,1)S(1)}, bf16[256,1024]{1,0:T(8,128)(2,1)S(1)}, bf16[256,1024]{1,0:T(8,128)(2,1)S(1)}, f32[8,320]{1,0:T(8,128)S(1)}) custom-call(bf16[256,1024]{1,0:T(8,128)(2,1)} %q_hbm.1, bf16[256,1024]{1,0:T(8,128)(2,1)} %k_hbm.1, bf16[256,1024]{1,0:T(8,128)(2,1)} %v_hbm.1, bf16[256,1024]{1,0:T(8,128)(2,1)} %g_hbm.1, ...), custom_call_target="tpu_custom_call" | custom-call | tf_op jit(solution)/shard_map/pallas_call | solution.py:621
  70.2 1.2 %shard_map.103 = (bf16[256,1024]{1,0:T(8,128)(2,1)}, bf16[256,1024]{1,0:T(8,128)(2,1)}, bf16[256,1024]{1,0:T(8,128)(2,1)}, f32[8,320]{1,0:T(8,128)}) custom-call(bf16[256,1024]{1,0:T(8,128)(2,1)S(1)} %get-tuple-element.8.refs_0_, bf16[256,1024]{1,0:T(8,128)(2,1)S(1)} %get-tuple-element.9.refs_1_, bf16[256,1024]{1,0:T(8,128)(2,1)S(1)} %get-tuple-element.10.refs_2_, ...), custom_call_target="tpu_custom_call" | custom-call | tf_op jit(solution)/shard_map/pallas_call | solution.py:662

commit v6 on v5

--- a/solution.py
+++ b/solution.py
@@ -283,6 +283,34 @@
         for copy in loads(k):
             copy.start()
 
+    pl.semaphore_wait(barrier, greeted)
+
+    def await_loads(k):
+        for copy in loads(k):
+            copy.wait()
+
+    def send_kv(k):
+        @pl.when(has_nxt)
+        def _():
+            kv_copy(k, 0).start()
+
+    def send_qg(k):
+        @pl.when(has_prv)
+        def _():
+            qg_copy(HEADS - 1 - k, 0).start()
+
+    for copy in stat_loads:
+        copy.wait()
+
+    @pl.when(has_prv)
+    def _():
+        st_copy(0).start()
+
+    for k in range(2):
+        await_loads(k)
+        send_kv(k)
+        send_qg(k)
+    pl.loop(2, HEADS)(await_loads)
     table_load.wait()
     ext[...] = jnp.broadcast_to(table_ref[:, TABLE_LEN - 1 : TABLE_LEN], (HEADS, 512))
     ext[:, 0:TABLE_LEN] = table_ref[...]
@@ -307,34 +335,6 @@
         bias[h, 3] = flat
         bias[h, 4] = jnp.where(far_off, -FAR, flat)
 
-    pl.semaphore_wait(barrier, greeted)
-
-    def await_loads(k):
-        for copy in loads(k):
-            copy.wait()
-
-    def send_kv(k):
-        @pl.when(has_nxt)
-        def _():
-            kv_copy(k, 0).start()
-
-    def send_qg(k):
-        @pl.when(has_prv)
-        def _():
-            qg_copy(HEADS - 1 - k, 0).start()
-
-    for copy in stat_loads:
-        copy.wait()
-
-    @pl.when(has_prv)
-    def _():
-        st_copy(0).start()
-
-    for k in range(2):
-        await_loads(k)
-        send_kv(k)
-        send_qg(k)
-    pl.loop(2, HEADS)(await_loads)
 
     def clear(buffer, start, rows):
         @pl.loop(0, HEADS)
@@ -505,7 +505,7 @@
 
         @pl.when(k == GROUP - 1)
         def _():
-            pl.loop(GROUP, HEADS)(send_own)
+            pl.loop(GROUP, 6)(send_own)
 
         in_round(1, 2 * k < z_rounds, hear)
         in_round(1, 2 * k + 1 < z_rounds, tell)
@@ -544,10 +544,13 @@
                 half, row = h // GROUP, 3 * (h % GROUP)
                 tab_half[half, row : row + 3, :] = tab[h, 0:3, :]
             core_copy.start()
+            forward(4)
             core_copy.wait_recv()
             over_y.start(tab_half[at_core] + tab_core[...])
-            pl.loop(GROUP, 6)(forward)
+            send_own(6)
+            forward(5)
             over_z.start(over_y.total())
+            send_own(7)
             pl.loop(6, HEADS)(forward)
 
     over_row.receive()

time: 71.8 us -> 69.1 us (0.962)
  Pallas kernels: 70.8 us -> 68 us
    pallas_call x1, Pallas kernels: 69.6 us -> 66.8 us  [local(): pl.pallas_call(functools.partial(kernel, sp_size, tp_size), out_shape=sha...]
where the time goes in v6:
time: 69.1 us; the launch traced here: 68.6 us
  Pallas kernels  68 us (98%)
    pallas_call x1, Pallas kernels, local(): pl.pallas_call(functools.partial(kernel, sp_size, tp_size), out_shape=sha...  66.8 us

profile of v6, /device:TPU:1, one launch (start us, length us, event | category | flops | bytes accessed | tf_op | source)
XLA Modules:
  0.0 68.6 jit_solution(51767397555359690)
XLA Ops:
  0.6 66.8 %shard_map.102 = (bf16[256,1024]{1,0:T(8,128)(2,1)S(1)}, bf16[256,1024]{1,0:T(8,128)(2,1)S(1)}, bf16[256,1024]{1,0:T(8,128)(2,1)S(1)}, f32[8,320]{1,0:T(8,128)S(1)}) custom-call(bf16[256,1024]{1,0:T(8,128)(2,1)} %q_hbm.1, bf16[256,1024]{1,0:T(8,128)(2,1)} %k_hbm.1, bf16[256,1024]{1,0:T(8,128)(2,1)} %v_hbm.1, bf16[256,1024]{1,0:T(8,128)(2,1)} %g_hbm.1, ...), custom_call_target="tpu_custom_call" | custom-call | tf_op jit(solution)/shard_map/pallas_call | solution.py:624
  67.4 1.2 %shard_map.103 = (bf16[256,1024]{1,0:T(8,128)(2,1)}, bf16[256,1024]{1,0:T(8,128)(2,1)}, bf16[256,1024]{1,0:T(8,128)(2,1)}, f32[8,320]{1,0:T(8,128)}) custom-call(bf16[256,1024]{1,0:T(8,128)(2,1)S(1)} %get-tuple-element.8.refs_0_, bf16[256,1024]{1,0:T(8,128)(2,1)S(1)} %get-tuple-element.9.refs_1_, bf16[256,1024]{1,0:T(8,128)(2,1)S(1)} %get-tuple-element.10.refs_2_, ...), custom_call_target="tpu_custom_call" | custom-call | tf_op jit(solution)/shard_map/pallas_call | solution.py:665

commit v7 on v6

--- a/solution.py
+++ b/solution.py
@@ -229,10 +229,10 @@
     lines = (
         (at(at_z, y_low, at_core), at(at_z, y_high, at_core), y_size > 2, y_size > 1),
         (at(z_low, at_y, at_core), at(z_high, at_y, at_core), at_z > 0, at_z < z_size - 1),
+        (prv, nxt, has_prv, has_nxt),
     )
     near = [(nxt, has_nxt), (prv, has_prv)]
-    near += [(over_row.device(over_row.other(step)), True) for step in range(1, row_size)]
-    for low, high, has_low, has_high in lines:
+    for low, high, has_low, has_high in lines[:2]:
         near += [(low, has_low), (high, has_high)]
     greeted = sum(jnp.where(cond, 1, 0) for _, cond in near)
 
@@ -494,6 +494,7 @@
     def _(k):
         in_round(0, k < y_rounds, tell)
         in_round(1, 2 * k < z_rounds, tell)
+        in_round(2, k < row_size - 2, tell)
 
         @pl.when(k < GROUP)
         def _():
@@ -536,6 +537,7 @@
                 table_row(1, back)
 
         in_round(0, k < y_rounds, hear)
+        in_round(2, k < row_size - 2, hear)
         in_round(1, 2 * k + 1 < z_rounds, hear)
 
         @pl.when(k == GROUP)
@@ -643,7 +645,7 @@
                 pltpu.VMEM((core_size * tp_size,) + tiles, F32),
                 pltpu.SemaphoreType.DMA((4, HEADS)),
                 pltpu.SemaphoreType.DMA((3,)),
-                pltpu.SemaphoreType.REGULAR((4,)),
+                pltpu.SemaphoreType.REGULAR((6,)),
                 pltpu.SemaphoreType.DMA((2,)),
                 pltpu.SemaphoreType.DMA((y_size,)),
                 pltpu.SemaphoreType.DMA((y_size,)),

time: 69.1 us -> 68.1 us (0.986)
  Pallas kernels: 68 us -> 67.2 us
    pallas_call x1, Pallas kernels: 66.8 us -> 66 us  [local(): pl.pallas_call(functools.partial(kernel, sp_size, tp_size), out_shape=sha...]
where the time goes in v7:
time: 68.1 us; the launch traced here: 67.9 us
  Pallas kernels  67.2 us (99%)
    pallas_call x1, Pallas kernels, local(): pl.pallas_call(functools.partial(kernel, sp_size, tp_size), out_shape=sha...  66 us

profile of v7, /device:TPU:1, one launch (start us, length us, event | category | flops | bytes accessed | tf_op | source)
XLA Modules:
  0.0 67.9 jit_solution(2192438219889631718)
XLA Ops:
  0.6 66.0 %shard_map.102 = (bf16[256,1024]{1,0:T(8,128)(2,1)S(1)}, bf16[256,1024]{1,0:T(8,128)(2,1)S(1)}, bf16[256,1024]{1,0:T(8,128)(2,1)S(1)}, f32[8,320]{1,0:T(8,128)S(1)}) custom-call(bf16[256,1024]{1,0:T(8,128)(2,1)} %q_hbm.1, bf16[256,1024]{1,0:T(8,128)(2,1)} %k_hbm.1, bf16[256,1024]{1,0:T(8,128)(2,1)} %v_hbm.1, bf16[256,1024]{1,0:T(8,128)(2,1)} %g_hbm.1, ...), custom_call_target="tpu_custom_call" | custom-call | tf_op jit(solution)/shard_map/pallas_call | solution.py:626
  66.7 1.2 %shard_map.103 = (bf16[256,1024]{1,0:T(8,128)(2,1)}, bf16[256,1024]{1,0:T(8,128)(2,1)}, bf16[256,1024]{1,0:T(8,128)(2,1)}, f32[8,320]{1,0:T(8,128)}) custom-call(bf16[256,1024]{1,0:T(8,128)(2,1)S(1)} %get-tuple-element.8.refs_0_, bf16[256,1024]{1,0:T(8,128)(2,1)S(1)} %get-tuple-element.9.refs_1_, bf16[256,1024]{1,0:T(8,128)(2,1)S(1)} %get-tuple-element.10.refs_2_, ...), custom_call_target="tpu_custom_call" | custom-call | tf_op jit(solution)/shard_map/pallas_call | solution.py:667
